TPU v7x, 512 devices: a whole 4x4x16 slice. The times are simulated.
512 devices in a mesh: sp: 64 (over z, y), tp: 8 (over x, core).
Axes of the slice: x: 4, y: 4, z: 16, core: 2. Of those that a mesh axis runs over, the one named last changes fastest.
Arguments:
- tokens: bfloat16 [24576, 2048], P(('sp', 'tp')), may hold values from -6 to 6
- query_weight: bfloat16 [2048, 1024], P(None, 'tp'), may hold values from -0.125 to 0.125
- key_weight: bfloat16 [2048, 1024], P(None, 'tp'), may hold values from -0.125 to 0.125
- value_weight: bfloat16 [2048, 1024], P(None, 'tp'), may hold values from -0.125 to 0.125
- query_gain: float32 [64], replicated, may hold values from 0.5 to 16
- key_gain: float32 [64], replicated, may hold values from 0.5 to 16
- log_gate_total: float32 [24576, 16], P('sp', 'tp'), may hold values from -3510 to 0, as said below
- output_weight: bfloat16 [1024, 2048], P('tp'), may hold values from -0.1875 to 0.1875
Outputs:
- mixed: bfloat16 [24576, 2048], P(('sp', 'tp'))
Inputs may be any that keep to these rules, and one draw needn't show every extreme that they name: `log_gate_total`: each column never rises from one position to the next.
All inputs are finite; a program needn't handle non-finite values.
Results may differ from a plain program's by a relative error of at most 0.014.
The roundings to bfloat16 on the way count: a program that leaves them out, or rounds other values in their place, can miss the bound.
Values may be sent and summed in bfloat16 or wider, within the bound.
A program may use at most 64 MiB of HBM per device.

v0:
```python
import math

import jax
import jax.numpy as jnp
from jax import lax
from jax.sharding import PartitionSpec as P

NORM_EPS = 1e-06


def head_norm(raw, gain, head_count):
    row_count = raw.shape[0]
    split = raw.reshape(row_count, head_count, -1)
    scaled = split * lax.rsqrt(jnp.mean(split * split, axis=-1, keepdims=True) + NORM_EPS) * gain
    return scaled.reshape(row_count, -1).astype(jnp.bfloat16)


def on_device(
    tokens,
    query_weight,
    key_weight,
    value_weight,
    query_gain,
    key_gain,
    log_gate_total,
    output_weight,
):
    attn_width = query_weight.shape[1]
    head_count = log_gate_total.shape[1]
    head_size = attn_width // head_count
    shard_rows = log_gate_total.shape[0]
    half_rows = shard_rows // 2
    sp_index = lax.axis_index("sp")
    score_scale = head_size ** (-0.5)
    pieces = lax.all_gather(tokens, "tp", axis=0, tiled=True)
    query_part = head_norm(
        jnp.dot(pieces, query_weight, preferred_element_type=jnp.float32), query_gain, head_count
    )
    key_part = head_norm(
        jnp.dot(pieces, key_weight, preferred_element_type=jnp.float32), key_gain, head_count
    )
    value_part = jnp.dot(pieces, value_weight, preferred_element_type=jnp.float32).astype(
        jnp.bfloat16
    )
    joined = jnp.stack([query_part, key_part, value_part], axis=0)
    queries = joined[0]
    key_value = joined[1:]
    gates_all = lax.all_gather(log_gate_total, "sp", axis=0, tiled=True)
    offsets = jnp.arange(shard_rows, dtype=jnp.int32)
    query_pos = sp_index * shard_rows + offsets
    query_heads = queries.reshape(shard_rows, head_count, head_size)
    gate_rows = log_gate_total.T
    halves = []
    for lower in (0, half_rows):
        pos_half = query_pos[lower : lower + half_rows]
        halves.append(
            (
                query_heads[lower : lower + half_rows],
                pos_half,
                gate_rows[:, lower : lower + half_rows],
                jnp.max(pos_half),
            )
        )
    half_state = (
        jnp.full((head_count, half_rows), -1e30, jnp.float32),
        jnp.zeros((head_count, half_rows), jnp.float32),
        jnp.zeros((head_count, half_rows, head_size), jnp.float32),
    )
    carry = (half_state, half_state)
    piece = lax.all_gather(key_value, "sp", axis=1, tiled=True)
    piece_rows = piece.shape[1]
    block_rows = math.gcd(piece_rows, 3072)
    block_count = piece_rows // block_rows
    key_blocks = piece[0].reshape(block_count, block_rows, head_count, head_size)
    value_blocks = piece[1].reshape(block_count, block_rows, head_count, head_size)
    gate_blocks = gates_all.reshape(block_count, block_rows, head_count)

    def one_block(state, inputs):
        key_block, value_block, key_gate, block_index = inputs
        block_start = block_index * block_rows
        key_pos = block_start + jnp.arange(block_rows, dtype=jnp.int32)
        key_gate_rows = key_gate.T
        updated = []
        for half_index in range(2):
            query_half, pos_half, gate_half, last_half = halves[half_index]

            def compute(current):
                running_max, running_sum, running_out = current
                scores = (
                    jnp.einsum(
                        "thd,shd->hts", query_half, key_block, preferred_element_type=jnp.float32
                    )
                    * score_scale
                )
                scores = scores + gate_half[:, :, None] - key_gate_rows[:, None, :]
                scores = jnp.where(
                    key_pos[None, None, :] <= pos_half[None, :, None], scores, -jnp.inf
                )
                new_max = jnp.maximum(running_max, jnp.max(scores, axis=2))
                rescale = jnp.exp(running_max - new_max)
                probs = jnp.exp(scores - new_max[:, :, None])
                running_sum = running_sum * rescale + jnp.sum(probs, axis=2)
                running_out = running_out * rescale[:, :, None] + jnp.einsum(
                    "hts,shd->htd",
                    probs.astype(jnp.bfloat16),
                    value_block,
                    preferred_element_type=jnp.float32,
                )
                return (new_max, running_sum, running_out)

            def keep_state(current):
                return current

            updated.append(
                lax.cond(block_start <= last_half, compute, keep_state, state[half_index])
            )
        return ((updated[0], updated[1]), None)

    carry, unused = lax.scan(
        one_block,
        carry,
        (key_blocks, value_blocks, gate_blocks, jnp.arange(block_count, dtype=jnp.int32)),
    )
    early_state, late_state = carry
    running_sum = jnp.concatenate([early_state[1], late_state[1]], axis=1)
    running_out = jnp.concatenate([early_state[2], late_state[2]], axis=1)
    attended = (
        (running_out / running_sum[:, :, None])
        .transpose(1, 0, 2)
        .reshape(shard_rows, attn_width)
        .astype(jnp.bfloat16)
    )
    mixed = lax.psum_scatter(
        jnp.dot(attended, output_weight, preferred_element_type=jnp.float32).astype(jnp.bfloat16),
        "tp",
        scatter_dimension=0,
        tiled=True,
    )
    return mixed


def solution(mesh):
    placed = (
        P(("sp", "tp"), None),
        P(None, "tp"),
        P(None, "tp"),
        P(None, "tp"),
        P(),
        P(),
        P("sp", "tp"),
        P("tp", None),
    )
    return jax.shard_map(
        on_device, mesh=mesh, in_specs=placed, out_specs=P(("sp", "tp"), None), check_vma=False
    )
```

profile of v0, /device:TPU:8, one launch (start us, length us, event | category | flops | bytes accessed | tf_op | source)
XLA Modules:
  0.0 410.6 jit_solution(5995559045676543723)
XLA Ops:
  8.1 37.8 %all-gather.3.cloned.1.call-done = bf16[384,2048]{1,0:T(8,128)(2,1)} async-done(((bf16[48,2048]{1,0:T(8,128)(2,1)}), bf16[384,2048]{1,0:T(8,128)(2,1)}) %all-gather.3.cloned.1.call-update) | async-done | bytes 1572880 | tf_op jit(solution)/shard_map/all_gather | solution.py:35
  45.8 2.2 bitcast_reduce_fusion.1
  48.2 2.1 fusion.16
  51.1 88.5 %all_gather.11 = f32[24576,2]{0,1:T(2,128)} all-gather(f32[384,2]{0,1:T(2,128)S(1)} %copy-done.5), channel_id=1, replica_groups=mesh['sp'=64,'tp'=8] {'sp'}, dimensions={0}, use_global_device_ids=true | all-gather | bytes 199680 | tf_op jit(solution)/shard_map/all_gather | solution.py:48
  143.0 96.8 %all-gather.5.cloned.1.call-done = bf16[2,24576,128]{1,2,0:T(8,128)(2,1)} async-done(((bf16[2,384,128]{1,2,0:T(8,128)(2,1)}), bf16[2,24576,128]{1,2,0:T(8,128)(2,1)}) %all-gather.5.cloned.1.call-update) | async-done | bytes 12582928 | tf_op jit(solution)/shard_map/all_gather | solution.py:70
  239.7 5.6 %fusion.22 = (bf16[1,24576,128]{1,2,0:T(8,128)(2,1)S(1)}, bf16[1,24576,128]{1,2,0:T(8,128)(2,1)S(1)}) fusion(bf16[2,24576,128]{1,2,0:T(8,128)(2,1)} %all-gather.5.cloned.1.call-done), kind=kLoop, calls=%fused_computation.44 | loop fusion | bytes 25165824 | tf_op jit(solution)/shard_map/slice | solution.py:75
  245.3 4.2 %copy.24 = bf16[16,8,8,3072]{3,2,1,0:T(8,128)(2,1)S(1)} copy(bf16[16,8,8,3072]{3,1,2,0:T(8,128)(2,1)S(1)} %bitcast.65) | data formatting | bytes 12582912
  249.5 6.1 %copy.21 = bf16[8,3072,2,64]{1,3,2,0:T(8,128)(2,1)} copy(bf16[8,3072,2,64]{1,0,3,2:T(8,128)(2,1)S(1)} %bitcast.62) | data formatting | bytes 12582912 | tf_op jit(solution)/shard_map/while | solution.py:119
  255.6 4.4 %copy.23 = bf16[16,8,8,3072]{3,2,1,0:T(8,128)(2,1)S(1)} copy(bf16[16,8,8,3072]{3,1,2,0:T(8,128)(2,1)S(1)} %bitcast.64) | data formatting | bytes 12582912
  260.0 6.1 %copy.20 = bf16[8,3072,2,64]{1,3,2,0:T(8,128)(2,1)} copy(bf16[8,3072,2,64]{1,0,3,2:T(8,128)(2,1)S(1)} %bitcast.63) | data formatting | bytes 12582912 | tf_op jit(solution)/shard_map/while | solution.py:119
  266.2 46.5 %while.20 = (s32[]{:T(128)}, f32[2,192]{1,0:T(2,128)S(1)}, f32[2,192]{1,0:T(2,128)S(1)}, f32[2,192,64]{1,2,0:T(8,128)S(1)}, f32[2,192]{1,0:T(2,128)S(1)}, /*inde...) while((s32[]{:T(128)}, f32[2,192]{1,0:T(2,128)S(1)}, ...), condition=%wide.region_13.14_spmd, body=%wide.region_4.13_spmd.sunk | while | flops 626496000 | bytes 37643284 | solution.py:119
  269.5 1.5 dynamic-slice_bitcast_fusion.5
  271.0 3.8 conditional.4
  271.4 1.6 fusion.20
  274.9 3.8 conditional.5
  275.3 1.6 fusion.21
  282.0 1.5 dynamic-slice_bitcast_fusion.5
  286.9 1.5 dynamic-slice_bitcast_fusion.5
  296.6 1.5 dynamic-slice_bitcast_fusion.5
  301.5 1.5 dynamic-slice_bitcast_fusion.5
  306.3 1.5 dynamic-slice_bitcast_fusion.5
  311.2 1.5 dynamic-slice_bitcast_fusion.5
  312.9 1.7 convolution_convert_fusion
  314.6 89.4 %reduce-scatter.2.cloned.1.call-done = bf16[48,2048]{1,0:T(8,128)(2,1)} async-done(((bf16[384,2048]{1,0:T(8,128)(2,1)}), bf16[48,2048]{1,0:T(8,128)(2,1)}) %reduce-scatter.2.cloned.1.call-update) | async-done | bytes 196624 | tf_op jit(solution)/shard_map/reduce_scatter | solution.py:133
  (100 shorter events, 22.7 us)
Async XLA Ops:
  6.5 306.3 %copy-start = (bf16[128,2048]{1,0:T(8,128)(2,1)S(1)}, bf16[128,2048]{1,0:T(8,128)(2,1)}, u32[]{:S(2)}) copy-start(bf16[128,2048]{1,0:T(8,128)(2,1)} %param.21) | copy-start | bytes 1572868
  6.5 44.5 %copy-start.6 = (f32[64]{0:T(128)S(1)}, f32[64]{0:T(128)}, u32[]{:S(2)}) copy-start(f32[64]{0:T(128)} %param.18) | copy-start | bytes 772
  6.5 44.6 %copy-start.5 = (f32[384,2]{0,1:T(2,128)S(1)}, f32[384,2]{0,1:T(2,128)}, u32[]{:S(2)}) copy-start(f32[384,2]{0,1:T(2,128)} %param.20) | copy-start | bytes 9220
  6.5 134.0 %copy-start.2 = (bf16[2048,128]{1,0:T(8,128)(2,1)S(1)}, bf16[2048,128]{1,0:T(8,128)(2,1)}, u32[]{:S(2)}) copy-start(bf16[2048,128]{1,0:T(8,128)(2,1)} %param.15) | copy-start | bytes 1572868
  6.5 39.3 %all-gather.3.cloned.1.call-start = ((), (), s32[]{:S(2)}) async-start(), calls=%async_computation.1 | async-start | bytes 1769472 | tf_op jit(solution)/shard_map/all_gather | solution.py:35
  7.3 232.5 %all-gather.5.cloned.1.call-start = ((), (), s32[]{:S(2)}) async-start(), calls=%async_computation.2 | async-start | bytes 12779520 | tf_op jit(solution)/shard_map/all_gather | solution.py:70
  45.8 94.7 %copy-start.1 = (bf16[384,2048]{1,0:T(8,128)(2,1)S(1)}, bf16[384,2048]{1,0:T(8,128)(2,1)}, u32[]{:S(2)}) copy-start(bf16[384,2048]{1,0:T(8,128)(2,1)} %all-gather.3.cloned.1.call-done) | copy-start | bytes 4718596
  51.0 353.1 %reduce-scatter.2.cloned.1.call-start = ((), (), s32[]{:S(2)}) async-start(), calls=%async_computation.3 | async-start | bytes 1769472 | tf_op jit(solution)/shard_map/reduce_scatter | solution.py:133
  260.0 6.2 %copy-start.3 = (bf16[192,128]{0,1:T(8,128)(2,1)S(1)}, bf16[192,128]{0,1:T(8,128)(2,1)}, u32[]{:S(2)}) copy-start(bf16[192,128]{0,1:T(8,128)(2,1)} %copy.19) | copy-start | bytes 147460
  260.0 6.2 %copy-start.4 = (bf16[192,128]{0,1:T(8,128)(2,1)S(1)}, bf16[192,128]{0,1:T(8,128)(2,1)}, u32[]{:S(2)}) copy-start(bf16[192,128]{0,1:T(8,128)(2,1)} %copy.18) | copy-start | bytes 147460
Sparse Core Ops, SparseCore 0:
  9.5 36.3 all-gather.2
  51.1 188.5 all-gather.4
  314.8 89.2 reduce-scatter.1
where the time goes:
time: 412 us; the launch traced here: 411 us
  waiting for transfers between devices  225 us (55%)
  blocking collectives  88.5 us (21%)
  local copies, waits for them, and re-layouts  51.5 us (12%)
  loops' own time  16.4 us (4%)
  between operations  13.3 us (3%)
  matrix products  11.9 us (3%)
  other arithmetic  4.22 us (1%)
    all_gather x1, waiting for transfers between devices, on_device(): piece = lax.all_gather(key_value, 'sp', axis=1, tiled=True)  96.8 us
    reduce_scatter x1, waiting for transfers between devices, on_device(): lax.psum_scatter(jnp.dot(attended, output_weight, preferred_element_type=...  89.4 us
    all_gather x1, blocking collectives, on_device(): gates_all = lax.all_gather(log_gate_total, 'sp', axis=0, tiled=True)  88.5 us
    all_gather x1, waiting for transfers between devices, on_device(): pieces = lax.all_gather(tokens, 'tp', axis=0, tiled=True)  37.8 us
    another operation x1, loops' own time, on_device(): lax.scan(one_block, carry, (key_blocks, value_blocks, gate_blocks, jnp.ar...  16.1 us
    while x2, local copies, waits for them, and re-layouts, on_device(): lax.scan(one_block, carry, (key_blocks, value_blocks, gate_blocks, jnp.ar...  12.2 us
    squeeze x8, local copies, waits for them, and re-layouts, on_device(): lax.scan(one_block, carry, (key_blocks, value_blocks, gate_blocks, jnp.ar...  11.8 us
    unnamed x16, local copies, waits for them, and re-layouts  8.62 us
  transfers between devices with their start and end apart: 3, of which 3 were waited for; matrix products, arithmetic and copies ran while one was open for 1% of the time, Pallas kernels for 0%

commit v1 on v0

v1 whole, which is shorter than its diff:
```python
import functools

import jax
import jax.numpy as jnp
from jax import lax
from jax.experimental import pallas as pl
from jax.experimental.pallas import tpu as pltpu
from jax.sharding import PartitionSpec as P

NORM_EPS = 1e-06
MESH = pl.DeviceIdType.MESH
F32 = jnp.float32
BF16 = jnp.bfloat16
LANES = 128
HEAD = 64
NX = 4
NY = 4
NC = 2
SUB = 256
QT = 256


class RowGather:
    def __init__(self, buf, rows, x, c, ids, ssem, rsem):
        self.buf, self.rows, self.x, self.c = buf, rows, x, c
        self.right, self.left, self.partner = ids
        self.ssem, self.rsem = ssem, rsem
        self.half = buf.shape[1] // 2

    def piece(self, dx, core, part):
        slot = lax.rem(self.x + dx + NX, NX) * NC + core
        rows = pl.ds(pl.multiple_of(slot * self.rows, self.rows), self.rows)
        if part is None:
            return self.buf.at[rows]
        return self.buf.at[rows, pl.ds(part * self.half, self.half)]

    def copy(self, dx, core, part, index):
        device = self.right if index < 3 else self.left if index < 6 else self.partner
        piece = self.piece(dx, core, part)
        return pltpu.make_async_remote_copy(
            src_ref=piece,
            dst_ref=piece,
            send_sem=self.ssem.at[index],
            recv_sem=self.rsem.at[index],
            device_id=device,
            device_id_type=MESH,
        )

    def send(self, dx, part, index):
        self.copy(dx, self.c, part, index).start()

    def arrive(self, dx, core, part, index):
        self.copy(dx, core, part, index).wait_recv()

    def start(self):
        self.send(0, 0, 0)
        self.send(0, 1, 3)
        self.send(0, 1, 1)
        self.send(0, 0, 4)
        self.send(0, None, 6)

    def relay(self):
        self.arrive(-1, self.c, 0, 0)
        self.send(-1, 0, 2)
        self.arrive(1, self.c, 1, 3)
        self.send(1, 1, 5)
        self.send(-1, 0, 7)
        self.send(1, 1, 8)

    def finish_links(self):
        self.arrive(-1, self.c, 1, 1)
        self.send(-1, 1, 9)
        self.arrive(1, self.c, 0, 4)
        self.send(1, 0, 10)
        self.arrive(-2, self.c, 0, 2)
        self.send(-2, 0, 11)
        self.arrive(2, self.c, 1, 5)
        self.send(2, 1, 12)

    def finish(self):
        other = 1 - self.c
        self.arrive(0, other, None, 6)
        self.arrive(-1, other, 0, 7)
        self.arrive(1, other, 1, 8)
        self.arrive(-1, other, 1, 9)
        self.arrive(1, other, 0, 10)
        self.arrive(-2, other, 0, 11)
        self.arrive(2, other, 1, 12)

    def drain(self):
        sent = [(0, 0, 0), (0, 1, 3), (0, 1, 1), (0, 0, 4), (0, None, 6), (-1, 0, 2), (1, 1, 5)]
        sent += [(-1, 0, 7), (1, 1, 8), (-1, 1, 9), (1, 0, 10), (-2, 0, 11), (2, 1, 12)]
        for dx, part, index in sent:
            self.copy(dx, self.c, part, index).wait_send()


def kernel(
    nz,
    tokens_ref,
    wq_ref,
    wk_ref,
    wv_ref,
    qgain_ref,
    kgain_ref,
    gates_ref,
    wout_ref,
    out_ref,
    tok,
    wqkv,
    wout,
    raw,
    kv_send,
    q_send,
    q_recv,
    gate_recv,
    kv_all,
    gate_all,
    q_s,
    gt_s,
    m_s,
    o_s,
    v_s,
    att_send,
    att_recv,
    lsem,
    tok_ss,
    tok_rs,
    wo_ss,
    wo_rs,
    a2a_ss,
    a2a_rs,
    ring_ss,
    ring_rs,
    d2d_ss,
    d2d_rs,
    gring_ss,
    gring_rs,
    gd2d_ss,
    gd2d_rs,
    own_ss,
    own_rs,
    att_ss,
    att_rs,
):
    sp = lax.axis_index("sp")
    tp = lax.axis_index("tp")
    z, y = lax.div(sp, NY), lax.rem(sp, NY)
    x, c = lax.div(tp, NC), lax.rem(tp, NC)

    def device(dz, dy, dx, dc):
        return (dz * NY + dy, dx * NC + dc)

    right = device(z, y, lax.rem(x + 1, NX), c)
    left = device(z, y, lax.rem(x + NX - 1, NX), c)
    partner = device(z, y, x, 1 - c)
    up = device(lax.rem(z + 1, nz), y, x, c)
    down = device(lax.rem(z + nz - 1, nz), y, x, c)
    owner_core = lax.div(y, 2)

    rows_tp = tokens_ref.shape[0]
    blk = rows_tp * NX * NC
    half = 2 * blk
    width = wq_ref.shape[1]

    own_rows = pl.ds(pl.multiple_of(tp * rows_tp, rows_tp), rows_tp)
    wout_rows = wout_ref.shape[0]
    load_tok = pltpu.make_async_copy(tokens_ref, tok.at[own_rows], lsem.at[0])
    load_tok.start()
    loads = []
    for i, w_ref in enumerate((wq_ref, wk_ref, wv_ref)):
        loads.append(
            pltpu.make_async_copy(w_ref, wqkv.at[:, pl.ds(i * width, width)], lsem.at[1 + i])
        )
    load_wout = pltpu.make_async_copy(
        wout_ref,
        wout.at[pl.ds(pl.multiple_of(tp * wout_rows, wout_rows), wout_rows)],
        lsem.at[4],
    )
    for load in loads:
        load.start()
    load_wout.start()

    barrier = pltpu.get_barrier_semaphore()
    for neighbour in (right, left, partner, up, down):
        pl.semaphore_signal(barrier, inc=1, device_id=neighbour, device_id_type=MESH)
    for i in range(2):
        j = 2 * c + i

        @pl.when(j != y)
        def _():
            pl.semaphore_signal(
                barrier, inc=1, device_id=device(z, j, x, owner_core), device_id_type=MESH
            )

    @pl.when(owner_core == c)
    def _():
        pl.semaphore_wait(barrier, 6)

    @pl.when(owner_core != c)
    def _():
        pl.semaphore_wait(barrier, 7)

    load_tok.wait()
    tok_gather = RowGather(tok, rows_tp, x, c, (right, left, partner), tok_ss, tok_rs)
    tok_gather.start()
    tok_gather.relay()
    tok_gather.finish_links()
    load_wout.wait()
    wout_gather = RowGather(wout, wout_rows, x, c, (right, left, partner), wo_ss, wo_rs)
    wout_gather.start()
    for load in loads:
        load.wait()
    tok_gather.finish()

    lane = lax.broadcasted_iota(jnp.int32, (LANES, LANES), 1)
    low = lane < HEAD

    qgain = qgain_ref[0:1, :]
    kgain = kgain_ref[0:1, :]

    def head_norm(raw_part, gain):
        square = raw_part * raw_part
        lo = jnp.sum(jnp.where(low, square, 0.0), axis=1, keepdims=True) * (1.0 / HEAD)
        hi = jnp.sum(jnp.where(low, 0.0, square), axis=1, keepdims=True) * (1.0 / HEAD)
        inverse = jnp.where(low, lax.rsqrt(lo + NORM_EPS), lax.rsqrt(hi + NORM_EPS))
        return raw_part * inverse * gain

    @pl.loop(0, blk // LANES)
    def _(t):
        rows = pl.ds(pl.multiple_of(t * LANES, LANES), LANES)
        raw[...] = jnp.dot(tok[rows, :], wqkv[...], preferred_element_type=F32)
        q_part = head_norm(raw[:, 0:width], qgain) * (HEAD**-0.5)
        k_part = head_norm(raw[:, width : 2 * width], kgain)
        v_part = raw[:, 2 * width : 3 * width]
        k_roll = pltpu.roll(k_part, HEAD, 1)
        v_roll = pltpu.roll(v_part, HEAD, 1)
        q_send[0, rows, :] = jnp.where(low, q_part, 0.0).astype(BF16)
        q_send[1, rows, :] = jnp.where(low, pltpu.roll(q_part, HEAD, 1), 0.0).astype(BF16)
        kv_send[0, rows, :] = jnp.where(low, k_part, v_roll).astype(BF16)
        kv_send[1, rows, :] = jnp.where(low, k_roll, v_part).astype(BF16)

    par = lax.rem(y, 2)
    a2a = []
    for i in range(2):
        j = 2 * c + i
        target = device(z, j, x, owner_core)
        own_block = kv_all.at[z, pl.ds(pl.multiple_of(y * blk, blk), blk)]
        parts = (
            (kv_send.at[i], own_block),
            (q_send.at[i], q_recv.at[par]),
            (gates_ref.at[i], gate_recv.at[par]),
        )
        for n, (src, dst) in enumerate(parts):
            send_sem, recv_sem = a2a_ss.at[n, i], a2a_rs.at[n, par]
            remote = pltpu.make_async_remote_copy(
                src_ref=src,
                dst_ref=dst,
                send_sem=send_sem,
                recv_sem=recv_sem,
                device_id=target,
                device_id_type=MESH,
            )
            local = pltpu.make_async_copy(src, dst, recv_sem)

            @pl.when(j != y)
            def _():
                remote.start()

            @pl.when(j == y)
            def _():
                local.start()

            a2a.append((j, remote))

    base = c * half
    for s in range(2):
        src_rows = pl.ds(pl.multiple_of(base + s * blk, blk), blk)
        for n, dst in enumerate((kv_all.at[z, src_rows], q_recv.at[s], gate_recv.at[s])):
            pltpu.make_async_copy(dst, dst, a2a_rs.at[n, s]).wait()

    gate_all[z, c] = gate_recv[0] + gate_recv[1]
    subs = half // SUB

    def kv_piece(b, core, s):
        return kv_all.at[b, pl.ds(pl.multiple_of(core * half + s * SUB, SUB), SUB)]

    def ring_copy(d, b, s, k, target):
        piece = kv_piece(b, c, s)
        return pltpu.make_async_remote_copy(
            src_ref=piece,
            dst_ref=piece,
            send_sem=ring_ss.at[d, k - 1, s],
            recv_sem=ring_rs.at[d, k - 1, s],
            device_id=target,
            device_id_type=MESH,
        )

    def ring_gate(d, b, k, target):
        piece = gate_all.at[b, c]
        return pltpu.make_async_remote_copy(
            src_ref=piece,
            dst_ref=piece,
            send_sem=gring_ss.at[d, k - 1],
            recv_sem=gring_rs.at[d, k - 1],
            device_id=target,
            device_id_type=MESH,
        )

    def d2d_copy(d, b, core, s, k):
        piece = kv_piece(b, core, s)
        return pltpu.make_async_remote_copy(
            src_ref=piece,
            dst_ref=piece,
            send_sem=d2d_ss.at[d, k - 1, s],
            recv_sem=d2d_rs.at[d, k - 1, s],
            device_id=partner,
            device_id_type=MESH,
        )

    def d2d_gate(d, b, core, k):
        piece = gate_all.at[b, core]
        return pltpu.make_async_remote_copy(
            src_ref=piece,
            dst_ref=piece,
            send_sem=gd2d_ss.at[d, k - 1],
            recv_sem=gd2d_rs.at[d, k - 1],
            device_id=partner,
            device_id_type=MESH,
        )

    k_up = nz // 2
    k_down = nz - 1 - k_up
    last_wrapped = k_down - 1
    links = (up, down)

    def block_of(d, k):
        return z - k if d == 0 else lax.rem(z + k, nz)

    def receives(d, k):
        if d == 0:
            return jnp.logical_and(z - k >= 0, k <= k_up)
        return jnp.logical_and(block_of(1, k) <= last_wrapped, k <= k_down)

    def sends(d, k):
        if d == 0:
            return jnp.logical_and(
                jnp.logical_and(z - k + 1 >= 0, z <= nz - 2), k <= k_up
            )
        return jnp.logical_and(block_of(1, k - 1) <= last_wrapped, k <= k_down)

    def needs(d, k):
        if d == 0:
            return receives(0, k)
        return jnp.logical_and(receives(1, k), block_of(1, k) < z)

    def own_copy(core, s):
        piece = kv_piece(z, core, s)
        return pltpu.make_async_remote_copy(
            src_ref=piece,
            dst_ref=piece,
            send_sem=own_ss.at[s],
            recv_sem=own_rs.at[s],
            device_id=partner,
            device_id_type=MESH,
        )

    def own_gate(core):
        piece = gate_all.at[z, core]
        return pltpu.make_async_remote_copy(
            src_ref=piece,
            dst_ref=piece,
            send_sem=own_ss.at[subs],
            recv_sem=own_rs.at[subs],
            device_id=partner,
            device_id_type=MESH,
        )

    for s in range(subs):
        for d in range(2):

            @pl.when(sends(d, 1))
            def _():
                if s == 0:
                    ring_gate(d, z, 1, links[d]).start()
                ring_copy(d, z, s, 1, links[d]).start()

        own_copy(c, s).start()
    own_gate(c).start()

    gate_t = jnp.transpose(gate_all[z, c])
    tiles_blk = blk // LANES
    for s in range(2):
        q_s[pl.ds(s * blk, blk), :] = q_recv[s]
    for t in range(2 * tiles_blk):
        column = gate_t[:, t : t + 1]
        gt_s[pl.ds(t * LANES, LANES), :] = jnp.broadcast_to(column, (LANES, LANES))
    m_s[...] = jnp.full(m_s.shape, -1e30, F32)
    o_s[...] = jnp.zeros(o_s.shape, F32)

    lane_row = lax.broadcasted_iota(jnp.int32, (1, LANES), 1)
    ones_low = jnp.where(lane_row < HEAD, 1.0, 0.0).astype(BF16)
    keep_high = jnp.where(lane_row < HEAD, 0.0, 1.0).astype(BF16)
    lane_tiles = SUB // LANES

    def update(q_tile, pieces, masked_at=None):
        rows = pl.ds(pl.multiple_of(q_tile * QT, QT), QT)
        query = q_s[rows, :]
        gt = gt_s[rows, :]
        m_old = m_s[rows, :]
        scores = []
        peak = None
        for key, gate_row, value in pieces:
            score = lax.dot_general(
                query, key, (((1,), (1,)), ((), ())), preferred_element_type=F32
            )
            score = score - gate_row
            if masked_at is not None:
                row_id, col_id = masked_at
                score = jnp.where(
                    lax.broadcasted_iota(jnp.int32, score.shape, 1) + col_id
                    <= lax.broadcasted_iota(jnp.int32, score.shape, 0) + row_id,
                    score,
                    -jnp.inf,
                )
            scores.append(score)
            top = jnp.max(score, axis=1, keepdims=True)
            peak = top if peak is None else jnp.maximum(peak, top)
        m_new = jnp.maximum(m_old, peak + gt)
        offset = m_new - gt
        wide = jnp.concatenate([offset] * lane_tiles, axis=1)
        total = o_s[rows, :] * jnp.exp(m_old - m_new)
        for (key, gate_row, value), score in zip(pieces, scores):
            probs = jnp.exp(score - wide).astype(BF16)
            total = total + jnp.dot(probs, value, preferred_element_type=F32)
        o_s[rows, :] = total
        m_s[rows, :] = m_new

    def gate_row_of(b, core, s):
        return jnp.concatenate(
            [gate_all[b, core, pl.ds(s * lane_tiles + i, 1), :] for i in range(lane_tiles)],
            axis=1,
        )

    for s in range(subs):
        own_copy(1 - c, s).wait_recv()
    own_gate(1 - c).wait_recv()
    for core in range(2):
        for s in range(subs):

            @pl.when(core <= c)
            def _():
                key = kv_all[z, pl.ds(core * half + s * SUB, SUB), :]
                value = key * keep_high + ones_low
                gate_row = gate_row_of(z, core, s)
                col_id = core * half + s * SUB

                @pl.loop(0, half // QT)
                def _(t):
                    row_id = c * half + t * QT

                    @pl.when(row_id + QT > col_id)
                    def _():
                        update(t, [(key, gate_row, value)], (row_id, col_id))

    def one_chunk(d, k, s):
        @pl.when(needs(d, k))
        def _():
            b = block_of(d, k)
            if s == 0:
                d2d_gate(d, b, 1 - c, k).wait_recv()
            d2d_copy(d, b, 1 - c, s, k).wait_recv()
            for core in range(2):
                key = kv_all[b, pl.ds(core * half + s * SUB, SUB), :]
                v_s[pl.ds(core * SUB, SUB), :] = key * keep_high + ones_low

            @pl.loop(0, half // QT)
            def _(t):
                update(
                    t,
                    [
                        (
                            kv_all[b, pl.ds(core * half + s * SUB, SUB), :],
                            gate_row_of(b, core, s),
                            v_s[pl.ds(core * SUB, SUB), :],
                        )
                        for core in range(2)
                    ],
                )

    def pass_on(d, k, s):
        @pl.when(receives(d, k))
        def _():
            b = block_of(d, k)
            if s == 0:
                ring_gate(d, b, k, links[d]).wait_recv()
            ring_copy(d, b, s, k, links[d]).wait_recv()

            @pl.when(sends(d, k + 1))
            def _():
                if s == 0:
                    ring_gate(d, b, k + 1, links[d]).start()
                ring_copy(d, b, s, k + 1, links[d]).start()

            @pl.when(needs(d, k))
            def _():
                if s == 0:
                    d2d_gate(d, b, c, k).start()
                d2d_copy(d, b, c, s, k).start()

    @pl.loop(1, k_up + 1)
    def _(k):
        for s in range(subs):
            pass_on(0, k, s)
            pass_on(1, k, s)
            if s == 0:

                @pl.when(k > 1)
                def _():
                    one_chunk(0, k - 1, subs - 1)
                    one_chunk(1, k - 1, subs - 1)

            else:
                one_chunk(0, k, s - 1)
                one_chunk(1, k, s - 1)

        @pl.when(k == k_up // 2)
        def _():
            wout_gather.relay()

        @pl.when(k == k_up - 1)
        def _():
            wout_gather.finish_links()

    one_chunk(0, k_up, subs - 1)
    one_chunk(1, k_up, subs - 1)

    odd = lax.rem(y, 2) == 1

    @pl.loop(0, half // LANES)
    def _(t):
        rows = pl.ds(pl.multiple_of(t * LANES, LANES), LANES)
        both = o_s[rows, :]
        swapped = pltpu.roll(both, HEAD, 1)

        @pl.when(odd)
        def _():
            att_send[rows, :] = jnp.where(low, 0.0, both / swapped).astype(BF16)

        @pl.when(jnp.logical_not(odd))
        def _():
            att_send[rows, :] = jnp.where(low, swapped / both, 0.0).astype(BF16)

    head = NY * x + y
    att = []
    for s in range(2):
        for t in range(NX * NC):
            ty = 2 * c + s
            src = att_send.at[pl.ds(s * blk + t * rows_tp, rows_tp)]
            remote = pltpu.make_async_remote_copy(
                src_ref=src,
                dst_ref=att_recv.at[head],
                send_sem=att_ss.at[s * NX * NC + t],
                recv_sem=att_rs.at[head],
                device_id=(z * NY + ty, t),
                device_id_type=MESH,
            )
            local = pltpu.make_async_copy(src, att_recv.at[head], att_rs.at[head])
            is_self = jnp.logical_and(ty == y, tp == t)

            @pl.when(jnp.logical_not(is_self))
            def _():
                remote.start()

            @pl.when(is_self)
            def _():
                local.start()

            att.append((is_self, remote))

    wout_gather.finish()
    for h in range(NX * NY):
        pltpu.make_async_copy(att_recv.at[h], att_recv.at[h], att_rs.at[h]).wait()

    groups = NX * NC
    pairs = [att_recv[2 * g] + att_recv[2 * g + 1] for g in range(groups)]
    cols = 256

    @pl.loop(0, out_ref.shape[1] // cols)
    def _(t):
        span = pl.ds(pl.multiple_of(t * cols, cols), cols)
        acc = jnp.zeros((rows_tp, cols), F32)
        for g in range(groups):
            part = jnp.dot(
                pairs[g],
                wout[pl.ds(g * wout_rows, wout_rows), span],
                preferred_element_type=F32,
            )
            acc = acc + part.astype(BF16).astype(F32)
        out_ref[:, span] = acc.astype(BF16)

    tok_gather.drain()
    wout_gather.drain()
    for j, remote in a2a:

        @pl.when(j != y)
        def _():
            remote.wait_send()

    for s in range(subs):
        own_copy(c, s).wait_send()
    own_gate(c).wait_send()

    @pl.loop(1, k_up + 1)
    def _(k):
        for d in range(2):

            @pl.when(sends(d, k))
            def _():
                b = block_of(d, k - 1)
                ring_gate(d, b, k, links[d]).wait_send()
                for s in range(subs):
                    ring_copy(d, b, s, k, links[d]).wait_send()

            @pl.when(needs(d, k))
            def _():
                b = block_of(d, k)
                d2d_gate(d, b, c, k).wait_send()
                for s in range(subs):
                    d2d_copy(d, b, c, s, k).wait_send()

    for is_self, remote in att:

        @pl.when(jnp.logical_not(is_self))
        def _():
            remote.wait_send()


def on_device(
    nz,
    tokens,
    query_weight,
    key_weight,
    value_weight,
    query_gain,
    key_gain,
    log_gate_total,
    output_weight,
):
    rows_tp, depth = tokens.shape
    width = query_weight.shape[1]
    blk, heads = log_gate_total.shape
    half = 2 * blk
    tiles = blk // LANES
    y = lax.rem(lax.axis_index("sp"), NY)
    rows = log_gate_total.T.reshape(heads, tiles, LANES)
    empty = jnp.zeros_like(rows)
    rest = jnp.zeros((heads, 8 - 2 * tiles, LANES), F32)
    odd = (y % 2) == 1
    gates = jnp.concatenate(
        [jnp.where(odd, empty, rows), jnp.where(odd, rows, empty), rest], axis=1
    )
    gain_rows = lambda gain: jnp.broadcast_to(jnp.concatenate([gain, gain])[None, :], (8, LANES))
    k_up = nz // 2
    subs = half // SUB
    dma = pltpu.SemaphoreType.DMA
    any_spec = pl.BlockSpec(memory_space=pl.ANY)
    vmem_spec = pl.BlockSpec(memory_space=pltpu.VMEM)
    return pl.pallas_call(
        functools.partial(kernel, nz),
        out_shape=jax.ShapeDtypeStruct((rows_tp, output_weight.shape[1]), BF16),
        in_specs=[any_spec] * 4 + [vmem_spec] * 3 + [any_spec],
        out_specs=vmem_spec,
        scratch_shapes=[
            pltpu.VMEM((blk, depth), BF16),
            pltpu.VMEM((depth, 3 * width), BF16),
            pltpu.VMEM((NX * NC * output_weight.shape[0], output_weight.shape[1]), BF16),
            pltpu.VMEM((LANES, 3 * width), F32),
            pltpu.VMEM((2, blk, LANES), BF16),
            pltpu.VMEM((2, blk, LANES), BF16),
            pltpu.VMEM((2, blk, LANES), BF16),
            pltpu.VMEM((2, 8, LANES), F32),
            pltpu.VMEM((nz, 2 * half, LANES), BF16),
            pltpu.VMEM((nz, 2, 8, LANES), F32),
            pltpu.VMEM((half, LANES), BF16),
            pltpu.VMEM((half, LANES), F32),
            pltpu.VMEM((half, LANES), F32),
            pltpu.VMEM((half, LANES), F32),
            pltpu.VMEM((2 * SUB, LANES), BF16),
            pltpu.VMEM((half, LANES), BF16),
            pltpu.VMEM((NX * NY, rows_tp, LANES), BF16),
            dma((5,)),
            dma((13,)),
            dma((13,)),
            dma((13,)),
            dma((13,)),
            dma((3, 2)),
            dma((3, 2)),
            dma((2, k_up, subs)),
            dma((2, k_up, subs)),
            dma((2, k_up, subs)),
            dma((2, k_up, subs)),
            dma((2, k_up)),
            dma((2, k_up)),
            dma((2, k_up)),
            dma((2, k_up)),
            dma((subs + 1,)),
            dma((subs + 1,)),
            dma((NX * NY,)),
            dma((NX * NY,)),
        ],
        compiler_params=pltpu.CompilerParams(
            collective_id=0, has_side_effects=True, vmem_limit_bytes=60 * 1024 * 1024
        ),
    )(
        tokens,
        query_weight,
        key_weight,
        value_weight,
        gain_rows(query_gain),
        gain_rows(key_gain),
        gates,
        output_weight,
    )


def solution(mesh):
    placed = (
        P(("sp", "tp"), None),
        P(None, "tp"),
        P(None, "tp"),
        P(None, "tp"),
        P(),
        P(),
        P("sp", "tp"),
        P("tp", None),
    )
    nz = mesh.shape["sp"] // NY
    return jax.shard_map(
        functools.partial(on_device, nz),
        mesh=mesh,
        in_specs=placed,
        out_specs=P(("sp", "tp"), None),
        check_vma=False,
    )
```

time: 412 us -> 115 us (0.28)
  the two profiles are of different devices: /device:TPU:8 before, /device:TPU:481 now
where the time goes in v1:
time: 115 us
  Pallas kernels  110 us (96%)
  local copies, waits for them, and re-layouts  4.24 us (4%)
    pallas_call x1, Pallas kernels, on_device(): pl.pallas_call(functools.partial(kernel, nz), out_shape=jax.ShapeDtypeStr...  110 us
    unnamed x7, local copies, waits for them, and re-layouts  2.95 us

profile of v1, /device:TPU:481, one launch (start us, length us, event | category | flops | bytes accessed | tf_op | source)
XLA Modules:
  0.0 114.6 jit_solution(12278935853379902933)
XLA Ops:
  0.0 0.0 copy-start.1
  0.0 0.7 copy-done.1
  0.7 0.0 copy-start.2
  0.7 0.1 pad_maximum_fusion
  0.7 0.6 copy-done.2
  1.3 0.1 pad_maximum_fusion.1
  1.4 0.1 pad.2.clone
  1.5 0.6 broadcast_in_dim.9.kgain_ref
  2.1 0.0 copy-start
  2.1 0.6 broadcast_in_dim.8.qgain_ref
  2.7 0.1 copy-done
  2.8 0.7 maximum_maximum_fusion.gates_ref
  3.5 109.5 %shard_map.82 = bf16[48,2048]{1,0:T(8,128)(2,1)} custom-call(bf16[48,2048]{1,0:T(8,128)(2,1)} %tokens_ref.1, bf16[2048,128]{1,0:T(8,128)(2,1)} %wq_ref.1, bf16[2048,128]{1,0:T(8,128)(2,1)} %wk_ref.1, bf16[2048,128]{1,0:T(8,128)(2,1)} %wv_ref.1, f32[8,128]{1,0:T(8,128)} %broadcast_in_dim.8.qgain_ref, f32[8,128]{1,0:T(8,128)} %broadcast_in_dim.9.kgain_ref, ...), custom_call_target="tpu_custom_call" | custom-call | tf_op jit(solution)/shard_map/pallas_call | solution.py:668
  113.0 1.6 %copy.10 = bf16[48,2048]{1,0:T(8,128)(2,1)} copy(bf16[48,2048]{1,0:T(8,128)(2,1)} %shard_map.82) | data formatting | bytes 393216
  (4 shorter events, 0.0 us)
Async XLA Ops:
  0.0 0.7 copy-start.1
  0.7 0.7 copy-start.2
  2.1 0.7 copy-start

commit v2 on v1

--- a/solution.py
+++ b/solution.py
@@ -16,8 +16,8 @@
 NX = 4
 NY = 4
 NC = 2
-SUB = 256
-QT = 256
+SUB = 384
+QT = 384
 
 
 class RowGather:
@@ -111,6 +111,9 @@
     raw,
     kv_send,
     q_send,
+    gain_v,
+    gate_v,
+    gate_send,
     q_recv,
     gate_recv,
     kv_all,
@@ -179,6 +182,12 @@
     for load in loads:
         load.start()
     load_wout.start()
+    smalls = []
+    for i, (src, dst) in enumerate(
+        ((qgain_ref, gain_v.at[0]), (kgain_ref, gain_v.at[1]), (gates_ref, gate_v))
+    ):
+        smalls.append(pltpu.make_async_copy(src, dst, lsem.at[5 + i]))
+        smalls[-1].start()
 
     barrier = pltpu.get_barrier_semaphore()
     for neighbour in (right, left, partner, up, down):
@@ -215,8 +224,18 @@
     lane = lax.broadcasted_iota(jnp.int32, (LANES, LANES), 1)
     low = lane < HEAD
 
-    qgain = qgain_ref[0:1, :]
-    kgain = kgain_ref[0:1, :]
+    for small in smalls:
+        small.wait()
+    qgain, kgain = [jnp.concatenate([gain_v[i], gain_v[i]], axis=1) for i in range(2)]
+    par = lax.rem(y, 2)
+    tiles_blk = blk // LANES
+    sublane = lax.broadcasted_iota(jnp.int32, (8, LANES), 0)
+    for i in range(2):
+        tile = jnp.zeros((8, LANES), F32)
+        for t in range(tiles_blk):
+            row = jnp.broadcast_to(gate_v[i : i + 1, t * LANES : (t + 1) * LANES], (8, LANES))
+            tile = jnp.where(sublane == par * tiles_blk + t, row, tile)
+        gate_send[i] = tile
 
     def head_norm(raw_part, gain):
         square = raw_part * raw_part
@@ -239,7 +258,6 @@
         kv_send[0, rows, :] = jnp.where(low, k_part, v_roll).astype(BF16)
         kv_send[1, rows, :] = jnp.where(low, k_roll, v_part).astype(BF16)
 
-    par = lax.rem(y, 2)
     a2a = []
     for i in range(2):
         j = 2 * c + i
@@ -248,7 +266,7 @@
         parts = (
             (kv_send.at[i], own_block),
             (q_send.at[i], q_recv.at[par]),
-            (gates_ref.at[i], gate_recv.at[par]),
+            (gate_send.at[i], gate_recv.at[par]),
         )
         for n, (src, dst) in enumerate(parts):
             send_sem, recv_sem = a2a_ss.at[n, i], a2a_rs.at[n, par]
@@ -384,11 +402,14 @@
                     ring_gate(d, z, 1, links[d]).start()
                 ring_copy(d, z, s, 1, links[d]).start()
 
-        own_copy(c, s).start()
-    own_gate(c).start()
+    @pl.when(c == 0)
+    def _():
+        for s in range(subs):
+            own_copy(c, s).start()
+        own_gate(c).start()
+
 
     gate_t = jnp.transpose(gate_all[z, c])
-    tiles_blk = blk // LANES
     for s in range(2):
         q_s[pl.ds(s * blk, blk), :] = q_recv[s]
     for t in range(2 * tiles_blk):
@@ -400,92 +421,72 @@
     lane_row = lax.broadcasted_iota(jnp.int32, (1, LANES), 1)
     ones_low = jnp.where(lane_row < HEAD, 1.0, 0.0).astype(BF16)
     keep_high = jnp.where(lane_row < HEAD, 0.0, 1.0).astype(BF16)
-    lane_tiles = SUB // LANES
-
-    def update(q_tile, pieces, masked_at=None):
-        rows = pl.ds(pl.multiple_of(q_tile * QT, QT), QT)
-        query = q_s[rows, :]
-        gt = gt_s[rows, :]
-        m_old = m_s[rows, :]
-        scores = []
-        peak = None
-        for key, gate_row, value in pieces:
+    tiles = half // QT
+
+    def update(b, cores, masked=False):
+        count = len(cores) * half
+        if count == 2 * half:
+            keys = lambda: kv_all[b]
+        else:
+            first = pl.multiple_of(cores[0] * half, half)
+            keys = lambda: kv_all[b, pl.ds(first, half), :]
+        v_s[pl.ds(0, count), :] = keys() * keep_high + ones_low
+        gate_row = jnp.concatenate(
+            [gate_all[b, core, pl.ds(i, 1), :] for core in cores for i in range(half // LANES)],
+            axis=1,
+        )
+
+        def score_of(t):
             score = lax.dot_general(
-                query, key, (((1,), (1,)), ((), ())), preferred_element_type=F32
+                q_s[pl.ds(t * QT, QT), :],
+                keys(),
+                (((1,), (1,)), ((), ())),
+                preferred_element_type=F32,
             )
             score = score - gate_row
-            if masked_at is not None:
-                row_id, col_id = masked_at
+            if masked:
+                shape = score.shape
+                row_id = lax.broadcasted_iota(jnp.int32, shape, 0) + t * QT
                 score = jnp.where(
-                    lax.broadcasted_iota(jnp.int32, score.shape, 1) + col_id
-                    <= lax.broadcasted_iota(jnp.int32, score.shape, 0) + row_id,
-                    score,
-                    -jnp.inf,
+                    lax.broadcasted_iota(jnp.int32, shape, 1) <= row_id, score, -jnp.inf
                 )
-            scores.append(score)
-            top = jnp.max(score, axis=1, keepdims=True)
-            peak = top if peak is None else jnp.maximum(peak, top)
-        m_new = jnp.maximum(m_old, peak + gt)
-        offset = m_new - gt
-        wide = jnp.concatenate([offset] * lane_tiles, axis=1)
-        total = o_s[rows, :] * jnp.exp(m_old - m_new)
-        for (key, gate_row, value), score in zip(pieces, scores):
+            return score
+
+        def add(t, score):
+            rows = pl.ds(t * QT, QT)
+            gt = gt_s[rows, :]
+            m_old = m_s[rows, :]
+            m_new = jnp.maximum(m_old, jnp.max(score, axis=1, keepdims=True) + gt)
+            wide = jnp.concatenate([m_new - gt] * (count // LANES), axis=1)
             probs = jnp.exp(score - wide).astype(BF16)
-            total = total + jnp.dot(probs, value, preferred_element_type=F32)
-        o_s[rows, :] = total
-        m_s[rows, :] = m_new
-
-    def gate_row_of(b, core, s):
-        return jnp.concatenate(
-            [gate_all[b, core, pl.ds(s * lane_tiles + i, 1), :] for i in range(lane_tiles)],
-            axis=1,
-        )
-
-    for s in range(subs):
-        own_copy(1 - c, s).wait_recv()
-    own_gate(1 - c).wait_recv()
-    for core in range(2):
+            o_s[rows, :] = o_s[rows, :] * jnp.exp(m_old - m_new) + jnp.dot(
+                probs, v_s[pl.ds(0, count), :], preferred_element_type=F32
+            )
+            m_s[rows, :] = m_new
+
+        score = score_of(0)
+        for t in range(tiles):
+            following = score_of(t + 1) if t + 1 < tiles else None
+            add(t, score)
+            score = following
+
+    update(z, (c,), masked=True)
+
+    @pl.when(c == 1)
+    def _():
         for s in range(subs):
-
-            @pl.when(core <= c)
-            def _():
-                key = kv_all[z, pl.ds(core * half + s * SUB, SUB), :]
-                value = key * keep_high + ones_low
-                gate_row = gate_row_of(z, core, s)
-                col_id = core * half + s * SUB
-
-                @pl.loop(0, half // QT)
-                def _(t):
-                    row_id = c * half + t * QT
-
-                    @pl.when(row_id + QT > col_id)
-                    def _():
-                        update(t, [(key, gate_row, value)], (row_id, col_id))
-
-    def one_chunk(d, k, s):
+            own_copy(0, s).wait_recv()
+        own_gate(0).wait_recv()
+        update(z, (1 - c,))
+
+    def one_block(d, k):
         @pl.when(needs(d, k))
         def _():
             b = block_of(d, k)
-            if s == 0:
-                d2d_gate(d, b, 1 - c, k).wait_recv()
-            d2d_copy(d, b, 1 - c, s, k).wait_recv()
-            for core in range(2):
-                key = kv_all[b, pl.ds(core * half + s * SUB, SUB), :]
-                v_s[pl.ds(core * SUB, SUB), :] = key * keep_high + ones_low
-
-            @pl.loop(0, half // QT)
-            def _(t):
-                update(
-                    t,
-                    [
-                        (
-                            kv_all[b, pl.ds(core * half + s * SUB, SUB), :],
-                            gate_row_of(b, core, s),
-                            v_s[pl.ds(core * SUB, SUB), :],
-                        )
-                        for core in range(2)
-                    ],
-                )
+            d2d_gate(d, b, 1 - c, k).wait_recv()
+            for s in range(subs):
+                d2d_copy(d, b, 1 - c, s, k).wait_recv()
+            update(b, (0, 1))
 
     def pass_on(d, k, s):
         @pl.when(receives(d, k))
@@ -512,16 +513,10 @@
         for s in range(subs):
             pass_on(0, k, s)
             pass_on(1, k, s)
-            if s == 0:
-
-                @pl.when(k > 1)
-                def _():
-                    one_chunk(0, k - 1, subs - 1)
-                    one_chunk(1, k - 1, subs - 1)
-
-            else:
-                one_chunk(0, k, s - 1)
-                one_chunk(1, k, s - 1)
+
+            @pl.when(k > 1)
+            def _():
+                one_block(s, k - 1)
 
         @pl.when(k == k_up // 2)
         def _():
@@ -531,8 +526,7 @@
         def _():
             wout_gather.finish_links()
 
-    one_chunk(0, k_up, subs - 1)
-    one_chunk(1, k_up, subs - 1)
+    one_block(0, k_up)
 
     odd = lax.rem(y, 2) == 1
 
@@ -606,9 +600,11 @@
         def _():
             remote.wait_send()
 
-    for s in range(subs):
-        own_copy(c, s).wait_send()
-    own_gate(c).wait_send()
+    @pl.when(c == 0)
+    def _():
+        for s in range(subs):
+            own_copy(c, s).wait_send()
+        own_gate(c).wait_send()
 
     @pl.loop(1, k_up + 1)
     def _(k):
@@ -650,16 +646,6 @@
     width = query_weight.shape[1]
     blk, heads = log_gate_total.shape
     half = 2 * blk
-    tiles = blk // LANES
-    y = lax.rem(lax.axis_index("sp"), NY)
-    rows = log_gate_total.T.reshape(heads, tiles, LANES)
-    empty = jnp.zeros_like(rows)
-    rest = jnp.zeros((heads, 8 - 2 * tiles, LANES), F32)
-    odd = (y % 2) == 1
-    gates = jnp.concatenate(
-        [jnp.where(odd, empty, rows), jnp.where(odd, rows, empty), rest], axis=1
-    )
-    gain_rows = lambda gain: jnp.broadcast_to(jnp.concatenate([gain, gain])[None, :], (8, LANES))
     k_up = nz // 2
     subs = half // SUB
     dma = pltpu.SemaphoreType.DMA
@@ -668,7 +654,7 @@
     return pl.pallas_call(
         functools.partial(kernel, nz),
         out_shape=jax.ShapeDtypeStruct((rows_tp, output_weight.shape[1]), BF16),
-        in_specs=[any_spec] * 4 + [vmem_spec] * 3 + [any_spec],
+        in_specs=[any_spec] * 8,
         out_specs=vmem_spec,
         scratch_shapes=[
             pltpu.VMEM((blk, depth), BF16),
@@ -677,6 +663,9 @@
             pltpu.VMEM((LANES, 3 * width), F32),
             pltpu.VMEM((2, blk, LANES), BF16),
             pltpu.VMEM((2, blk, LANES), BF16),
+            pltpu.VMEM((2, 1, HEAD), F32),
+            pltpu.VMEM((heads, blk), F32),
+            pltpu.VMEM((2, 8, LANES), F32),
             pltpu.VMEM((2, blk, LANES), BF16),
             pltpu.VMEM((2, 8, LANES), F32),
             pltpu.VMEM((nz, 2 * half, LANES), BF16),
@@ -685,10 +674,10 @@
             pltpu.VMEM((half, LANES), F32),
             pltpu.VMEM((half, LANES), F32),
             pltpu.VMEM((half, LANES), F32),
-            pltpu.VMEM((2 * SUB, LANES), BF16),
+            pltpu.VMEM((2 * half, LANES), BF16),
             pltpu.VMEM((half, LANES), BF16),
             pltpu.VMEM((NX * NY, rows_tp, LANES), BF16),
-            dma((5,)),
+            dma((8,)),
             dma((13,)),
             dma((13,)),
             dma((13,)),
@@ -716,9 +705,9 @@
         query_weight,
         key_weight,
         value_weight,
-        gain_rows(query_gain),
-        gain_rows(key_gain),
-        gates,
+        query_gain[None, :],
+        key_gain[None, :],
+        log_gate_total.T,
         output_weight,
     )
 

time: 115 us -> 79.6 us (0.69)
  the two profiles are of different devices: /device:TPU:481 before, /device:TPU:385 now
where the time goes in v2:
time: 79.6 us; the launch traced here: 79.5 us
  Pallas kernels  77.9 us (98%)
  local copies, waits for them, and re-layouts  1.62 us (2%)
    pallas_call x1, Pallas kernels, on_device(): pl.pallas_call(functools.partial(kernel, nz), out_shape=jax.ShapeDtypeStr...  77.9 us
    unnamed x1, local copies, waits for them, and re-layouts  1.62 us

profile of v2, /device:TPU:385, one launch (start us, length us, event | category | flops | bytes accessed | tf_op | source)
XLA Modules:
  0.0 79.5 jit_solution(939187565344174502)
XLA Ops:
  0.0 77.9 %shard_map.82 = bf16[48,2048]{1,0:T(8,128)(2,1)} custom-call(bf16[48,2048]{1,0:T(8,128)(2,1)} %tokens_ref.1, bf16[2048,128]{1,0:T(8,128)(2,1)} %wq_ref.1, bf16[2048,128]{1,0:T(8,128)(2,1)} %wk_ref.1, bf16[2048,128]{1,0:T(8,128)(2,1)} %wv_ref.1, f32[1,64]{1,0:T(1,128)} %bitcast.4, f32[1,64]{1,0:T(1,128)} %bitcast.5, f32[2,384]{1,0:T(2,128)} %bitcast.3, ...), custom_call_target="tpu_custom_call" | custom-call | tf_op jit(solution)/shard_map/pallas_call | solution.py:654
  77.9 1.6 %copy.10 = bf16[48,2048]{1,0:T(8,128)(2,1)} copy(bf16[48,2048]{1,0:T(8,128)(2,1)} %shard_map.82) | data formatting | bytes 393216

commit v3 on v2

v3 whole, which is shorter than its diff:
```python
import functools

import jax
import jax.numpy as jnp
from jax import lax
from jax.experimental import pallas as pl
from jax.experimental.pallas import tpu as pltpu
from jax.sharding import PartitionSpec as P

NORM_EPS = 1e-06
MESH = pl.DeviceIdType.MESH
F32 = jnp.float32
BF16 = jnp.bfloat16
LANES = 128
HEAD = 64
NX = 4
NY = 4
NC = 2
QT = 384


class RowGather:
    def __init__(self, buf, rows, x, c, ids, ssem, rsem):
        self.buf, self.rows, self.x, self.c = buf, rows, x, c
        self.right, self.left, self.partner = ids
        self.ssem, self.rsem = ssem, rsem
        self.half = buf.shape[1] // 2

    def piece(self, dx, core, part):
        slot = lax.rem(self.x + dx + NX, NX) * NC + core
        rows = pl.ds(pl.multiple_of(slot * self.rows, self.rows), self.rows)
        if part is None:
            return self.buf.at[rows]
        return self.buf.at[rows, pl.ds(part * self.half, self.half)]

    def copy(self, dx, core, part, index):
        device = self.right if index < 3 else self.left if index < 6 else self.partner
        piece = self.piece(dx, core, part)
        return pltpu.make_async_remote_copy(
            src_ref=piece,
            dst_ref=piece,
            send_sem=self.ssem,
            recv_sem=self.rsem.at[index],
            device_id=device,
            device_id_type=MESH,
        )

    def send(self, dx, part, index):
        self.copy(dx, self.c, part, index).start()

    def arrive(self, dx, core, part, index):
        self.copy(dx, core, part, index).wait_recv()

    def start(self):
        self.send(0, 0, 0)
        self.send(0, 1, 3)
        self.send(0, 1, 1)
        self.send(0, 0, 4)
        self.send(0, None, 6)

    def relay(self):
        self.arrive(-1, self.c, 0, 0)
        self.send(-1, 0, 2)
        self.arrive(1, self.c, 1, 3)
        self.send(1, 1, 5)
        self.send(-1, 0, 7)
        self.send(1, 1, 8)

    def finish_links(self):
        self.arrive(-1, self.c, 1, 1)
        self.send(-1, 1, 9)
        self.arrive(1, self.c, 0, 4)
        self.send(1, 0, 10)
        self.arrive(-2, self.c, 0, 2)
        self.send(-2, 0, 11)
        self.arrive(2, self.c, 1, 5)
        self.send(2, 1, 12)

    def finish(self):
        other = 1 - self.c
        self.arrive(0, other, None, 6)
        self.arrive(-1, other, 0, 7)
        self.arrive(1, other, 1, 8)
        self.arrive(-1, other, 1, 9)
        self.arrive(1, other, 0, 10)
        self.arrive(-2, other, 0, 11)
        self.arrive(2, other, 1, 12)

    def drain(self):
        sent = self.buf.at[pl.ds(0, 7 * self.rows)]
        pltpu.make_async_copy(sent, sent, self.ssem).wait()


def kernel(
    nz,
    tokens_ref,
    wq_ref,
    wk_ref,
    wv_ref,
    qgain_ref,
    kgain_ref,
    gates_ref,
    wout_ref,
    out_ref,
    tok,
    wqkv,
    wout,
    raw,
    kv_send,
    q_send,
    gain_v,
    gate_v,
    gate_send,
    q_recv,
    gate_recv,
    kv_all,
    gate_all,
    q_s,
    gt_s,
    m_s,
    o_s,
    v_s,
    att_send,
    att_recv,
    lsem,
    tok_ss,
    tok_rs,
    wo_ss,
    wo_rs,
    a2a_ss,
    a2a_rs,
    ring_ss,
    ring_rs,
    d2d_ss,
    d2d_rs,
    own_ss,
    own_rs,
    att_ss,
    att_rs,
):
    sp = lax.axis_index("sp")
    tp = lax.axis_index("tp")
    z, y = lax.div(sp, NY), lax.rem(sp, NY)
    x, c = lax.div(tp, NC), lax.rem(tp, NC)

    def device(dz, dy, dx, dc):
        return (dz * NY + dy, dx * NC + dc)

    right = device(z, y, lax.rem(x + 1, NX), c)
    left = device(z, y, lax.rem(x + NX - 1, NX), c)
    partner = device(z, y, x, 1 - c)
    up = device(lax.rem(z + 1, nz), y, x, c)
    down = device(lax.rem(z + nz - 1, nz), y, x, c)
    owner_core = lax.div(y, 2)

    rows_tp = tokens_ref.shape[0]
    blk = rows_tp * NX * NC
    half = 2 * blk
    width = wq_ref.shape[1]

    own_rows = pl.ds(pl.multiple_of(tp * rows_tp, rows_tp), rows_tp)
    wout_rows = wout_ref.shape[0]
    load_tok = pltpu.make_async_copy(tokens_ref, tok.at[own_rows], lsem.at[0])
    load_tok.start()
    loads = []
    for i, w_ref in enumerate((wq_ref, wk_ref, wv_ref)):
        loads.append(
            pltpu.make_async_copy(w_ref, wqkv.at[:, pl.ds(i * width, width)], lsem.at[1 + i])
        )
    load_wout = pltpu.make_async_copy(
        wout_ref,
        wout.at[pl.ds(pl.multiple_of(tp * wout_rows, wout_rows), wout_rows)],
        lsem.at[4],
    )
    for load in loads:
        load.start()
    load_wout.start()
    smalls = []
    for i, (src, dst) in enumerate(
        ((qgain_ref, gain_v.at[0]), (kgain_ref, gain_v.at[1]), (gates_ref, gate_v))
    ):
        smalls.append(pltpu.make_async_copy(src, dst, lsem.at[5 + i]))
        smalls[-1].start()

    barrier = pltpu.get_barrier_semaphore()
    for neighbour in (right, left, partner, up, down):
        pl.semaphore_signal(barrier, inc=1, device_id=neighbour, device_id_type=MESH)
    for i in range(2):
        j = 2 * c + i

        @pl.when(j != y)
        def _():
            pl.semaphore_signal(
                barrier, inc=1, device_id=device(z, j, x, owner_core), device_id_type=MESH
            )

    @pl.when(owner_core == c)
    def _():
        pl.semaphore_wait(barrier, 6)

    @pl.when(owner_core != c)
    def _():
        pl.semaphore_wait(barrier, 7)

    load_tok.wait()
    tok_gather = RowGather(tok, rows_tp, x, c, (right, left, partner), tok_ss, tok_rs)
    tok_gather.start()
    par = lax.rem(y, 2)
    tiles_blk = blk // LANES

    for small in smalls:
        small.wait()
    sublane = lax.broadcasted_iota(jnp.int32, (8, LANES), 0)
    for i in range(2):
        tile = jnp.zeros((8, LANES), F32)
        for t in range(tiles_blk):
            row = jnp.broadcast_to(gate_v[i : i + 1, t * LANES : (t + 1) * LANES], (8, LANES))
            tile = jnp.where(sublane == par * tiles_blk + t, row, tile)
        gate_send[i] = tile

    def exchange(n, i, src, dst):
        j = 2 * c + i
        remote = pltpu.make_async_remote_copy(
            src_ref=src,
            dst_ref=dst,
            send_sem=a2a_ss.at[n, i],
            recv_sem=a2a_rs.at[n, par],
            device_id=device(z, j, x, owner_core),
            device_id_type=MESH,
        )

        @pl.when(j != y)
        def _():
            remote.start()

        @pl.when(j == y)
        def _():
            pltpu.make_async_copy(src, dst, a2a_rs.at[n, par]).start()

        exchanged.append((j, remote))

    def received(n, s, dst):
        pltpu.make_async_copy(dst, dst, a2a_rs.at[n, s]).wait()

    exchanged = []
    for i in range(2):
        exchange(2, i, gate_send.at[i], gate_recv.at[par])

    tok_gather.relay()
    tok_gather.finish_links()
    load_wout.wait()
    wout_gather = RowGather(wout, wout_rows, x, c, (right, left, partner), wo_ss, wo_rs)
    wout_gather.start()
    for load in loads:
        load.wait()
    tok_gather.finish()

    lane = lax.broadcasted_iota(jnp.int32, (LANES, LANES), 1)
    low = lane < HEAD
    qgain, kgain = [jnp.concatenate([gain_v[i], gain_v[i]], axis=1) for i in range(2)]

    def head_norm(raw_part, gain):
        square = raw_part * raw_part
        lo = jnp.sum(jnp.where(low, square, 0.0), axis=1, keepdims=True) * (1.0 / HEAD)
        hi = jnp.sum(jnp.where(low, 0.0, square), axis=1, keepdims=True) * (1.0 / HEAD)
        inverse = jnp.where(low, lax.rsqrt(lo + NORM_EPS), lax.rsqrt(hi + NORM_EPS))
        return raw_part * inverse * gain

    raw[...] = jnp.dot(tok[...], wqkv[:, width : 3 * width], preferred_element_type=F32)
    for t in range(tiles_blk):
        rows = pl.ds(t * LANES, LANES)
        k_part = head_norm(raw[rows, 0:width], kgain)
        v_part = raw[rows, width : 2 * width]
        k_roll = pltpu.roll(k_part, HEAD, 1)
        v_roll = pltpu.roll(v_part, HEAD, 1)
        kv_send[0, rows, :] = jnp.where(low, k_part, v_roll).astype(BF16)
        kv_send[1, rows, :] = jnp.where(low, k_roll, v_part).astype(BF16)
    for i in range(2):
        exchange(0, i, kv_send.at[i], kv_all.at[z, par, owner_core])

    raw[:, 0:width] = jnp.dot(tok[...], wqkv[:, 0:width], preferred_element_type=F32)
    for t in range(tiles_blk):
        rows = pl.ds(t * LANES, LANES)
        raw[rows, width : 2 * width] = head_norm(raw[rows, 0:width], qgain) * (HEAD**-0.5)
    pack = blk // 2
    step = 64
    for t in range(pack // step):
        first = raw[pl.ds(t * step, step), width : 2 * width]
        second = raw[pl.ds(pack + t * step, step), width : 2 * width]
        rows = pl.ds(t * step, step)
        q_send[0, rows, :] = jnp.where(low[:step], first, pltpu.roll(second, HEAD, 1)).astype(BF16)
        q_send[1, rows, :] = jnp.where(low[:step], pltpu.roll(first, HEAD, 1), second).astype(BF16)
    for i in range(2):
        exchange(1, i, q_send.at[i], q_recv.at[par])

    subs = 2

    def chunk_copies(b, s, target, send_sem, recv_sem):
        pieces = (kv_all.at[b, s, c], gate_all.at[b, c])
        return [
            pltpu.make_async_remote_copy(
                src_ref=piece,
                dst_ref=piece,
                send_sem=send_sem,
                recv_sem=recv_sem,
                device_id=target,
                device_id_type=MESH,
            )
            for piece in (pieces if s == 0 else pieces[:1])
        ]

    def chunk_wait(s, sem):
        gate_rows = 8 * LANES * 4 // (LANES * 2)
        sized = v_s.at[pl.ds(0, blk + gate_rows if s == 0 else blk)]
        pltpu.make_async_copy(sized, sized, sem).wait()

    k_up = nz // 2
    links = (up, down)

    def block_of(d, k):
        return z - k if d == 0 else lax.rem(z + k, nz)

    def whole(d, k, s):
        return k <= (k_up if s == d else k_up - 1)

    def highest(s):
        return k_up - 1 if s == 1 else k_up - 2

    def receives(d, k, s):
        block = block_of(d, k)
        return jnp.logical_and(block >= 0 if d == 0 else block <= highest(s), whole(d, k, s))

    def sends(d, k, s):
        if d == 0:
            there = jnp.logical_and(z - k + 1 >= 0, z <= nz - 2)
        else:
            there = lax.rem(z + k - 1, nz) <= highest(s)
        return jnp.logical_and(there, whole(d, k, s))

    def needs(d, k, s):
        if d == 0:
            return receives(0, k, s)
        return jnp.logical_and(receives(1, k, s), block_of(1, k) < z)

    for s in range(subs):
        received(2, s, gate_recv.at[s])
    gate_all[z, c] = gate_recv[0] + gate_recv[1]
    for s in range(subs):
        received(0, s, kv_all.at[z, s, c])
        for d in range(2):

            @pl.when(sends(d, 1, s))
            def _():
                for copy in chunk_copies(z, s, links[d], ring_ss.at[d, s], ring_rs.at[d, 0, s]):
                    copy.start()

    @pl.when(c == 0)
    def _():
        for s in range(subs):
            for copy in chunk_copies(z, s, partner, own_ss.at[s], own_rs.at[s]):
                copy.start()

    gate_t = jnp.transpose(gate_all[z, c])
    for t in range(2 * tiles_blk):
        column = gate_t[:, t : t + 1]
        gt_s[pl.ds(t * LANES, LANES), :] = jnp.broadcast_to(column, (LANES, LANES))
    m_s[...] = jnp.full(m_s.shape, -1e30, F32)
    o_s[...] = jnp.zeros(o_s.shape, F32)
    for s in range(subs):
        received(1, s, q_recv.at[s])
        for t in range(pack // step):
            packed = q_recv[s, pl.ds(t * step, step), :].astype(F32)
            second = pltpu.roll(packed, HEAD, 1)
            for n, rows in enumerate((packed, second)):
                first_row = s * blk + n * pack + t * step
                q_s[pl.ds(first_row, step), :] = jnp.where(low[:step], rows, 0.0).astype(BF16)

    lane_row = lax.broadcasted_iota(jnp.int32, (1, LANES), 1)
    ones_low = jnp.where(lane_row < HEAD, 1.0, 0.0).astype(BF16)
    keep_high = jnp.where(lane_row < HEAD, 0.0, 1.0).astype(BF16)
    tiles = half // QT

    def update(pieces, masked=False):
        count = len(pieces) * blk

        def keys():
            return jnp.concatenate([kv_all[b, s, core] for b, s, core in pieces], axis=0)

        v_s[pl.ds(0, count), :] = keys() * keep_high + ones_low
        gate_row = jnp.concatenate(
            [
                gate_all[b, core, pl.ds(s * tiles_blk + i, 1), :]
                for b, s, core in pieces
                for i in range(tiles_blk)
            ],
            axis=1,
        )

        def score_of(t):
            score = lax.dot_general(
                q_s[pl.ds(t * QT, QT), :],
                keys(),
                (((1,), (1,)), ((), ())),
                preferred_element_type=F32,
            )
            score = score - gate_row
            if masked:
                shape = score.shape
                row_id = lax.broadcasted_iota(jnp.int32, shape, 0) + t * QT
                score = jnp.where(
                    lax.broadcasted_iota(jnp.int32, shape, 1) <= row_id, score, -jnp.inf
                )
            return score

        def add(t, score):
            rows = pl.ds(t * QT, QT)
            gt = gt_s[rows, :]
            m_old = m_s[rows, :]
            m_new = jnp.maximum(m_old, jnp.max(score, axis=1, keepdims=True) + gt)
            wide = jnp.concatenate([m_new - gt] * (count // LANES), axis=1)
            probs = jnp.exp(score - wide).astype(BF16)
            o_s[rows, :] = o_s[rows, :] * jnp.exp(m_old - m_new) + jnp.dot(
                probs, v_s[pl.ds(0, count), :], preferred_element_type=F32
            )
            m_s[rows, :] = m_new

        score = score_of(0)
        for t in range(tiles):
            following = score_of(t + 1) if t + 1 < tiles else None
            add(t, score)
            score = following

    update([(z, s, c) for s in range(subs)], masked=True)

    @pl.when(c == 1)
    def _():
        for s in range(subs):
            chunk_wait(s, own_rs.at[s])
        update([(z, s, 0) for s in range(subs)])

    def pieces_of(d, k, s):
        return [(block_of(d, k), s, core) for core in range(2)]

    def relayed(d, k, s):
        chunk_wait(s, d2d_rs.at[d, k - 1, s])

    def pair(k, s):
        @pl.when(needs(1, k, s))
        def _():
            relayed(0, k, s)
            relayed(1, k, s)
            update(pieces_of(0, k, s) + pieces_of(1, k, s))

        @pl.when(jnp.logical_and(needs(0, k, s), jnp.logical_not(needs(1, k, s))))
        def _():
            relayed(0, k, s)
            update(pieces_of(0, k, s))

    def pass_on(d, k, s):
        @pl.when(receives(d, k, s))
        def _():
            b = block_of(d, k)
            chunk_wait(s, ring_rs.at[d, k - 1, s])

            @pl.when(sends(d, k + 1, s))
            def _():
                @pl.when(sends(d, k, s))
                def _():
                    chunk_wait(s, ring_ss.at[d, s])

                for copy in chunk_copies(b, s, links[d], ring_ss.at[d, s], ring_rs.at[d, k, s]):
                    copy.start()

            @pl.when(needs(d, k, s))
            def _():
                @pl.when(jnp.logical_and(k > 1, needs(d, k - 1, s)))
                def _():
                    chunk_wait(s, d2d_ss.at[d, s])

                for copy in chunk_copies(
                    b, s, partner, d2d_ss.at[d, s], d2d_rs.at[d, k - 1, s]
                ):
                    copy.start()

    @pl.loop(1, k_up)
    def _(k):
        pass_on(0, k, 0)
        pass_on(1, k, 0)

        @pl.when(k > 1)
        def _():
            pair(k - 1, 1)

        pass_on(0, k, 1)
        pass_on(1, k, 1)
        pair(k, 0)

        @pl.when(k == 3)
        def _():
            wout_gather.relay()

        @pl.when(k == 5)
        def _():
            wout_gather.finish_links()

    for s in range(subs):
        pass_on(s, k_up, s)
    pair(k_up - 1, 1)

    @pl.when(z >= k_up)
    def _():
        for s in range(subs):
            relayed(s, k_up, s)
        update([(z - k_up, s, core) for s in range(subs) for core in range(2)])

    odd_head = lax.rem(y, 2) == 1
    few = rows_tp // 2

    for n in range(half // rows_tp):
        first = o_s[pl.ds(n * rows_tp, few), :]
        second = o_s[pl.ds(n * rows_tp + few, few), :]
        first = pltpu.roll(first, HEAD, 1) / first
        second = second / pltpu.roll(second, HEAD, 1)
        att_send[n] = jnp.where(low[:few], first, second).astype(BF16)

    head = NY * x + y
    att = []
    for s in range(subs):
        for t in range(NX * NC):
            ty = 2 * c + s
            src = att_send.at[s * NX * NC + t]
            remote = pltpu.make_async_remote_copy(
                src_ref=src,
                dst_ref=att_recv.at[head],
                send_sem=att_ss,
                recv_sem=att_rs,
                device_id=(z * NY + ty, t),
                device_id_type=MESH,
            )
            local = pltpu.make_async_copy(src, att_recv.at[head], att_rs)
            is_self = jnp.logical_and(ty == y, tp == t)

            @pl.when(jnp.logical_not(is_self))
            def _():
                remote.start()

            @pl.when(is_self)
            def _():
                local.start()

    wout_gather.finish()
    pltpu.make_async_copy(att_recv, att_recv, att_rs).wait()

    groups = NX * NC
    pairs = []
    for g in range(groups):
        even, odd = [att_recv[2 * g + n].astype(F32) for n in range(2)]
        early = jnp.where(low[:few], even, pltpu.roll(odd, HEAD, 1))
        late = jnp.where(low[:few], pltpu.roll(even, HEAD, 1), odd)
        pairs.append(jnp.concatenate([early, late], axis=0).astype(BF16))
    cols = 256

    @pl.loop(0, out_ref.shape[1] // cols)
    def _(t):
        span = pl.ds(pl.multiple_of(t * cols, cols), cols)
        acc = jnp.zeros((rows_tp, cols), F32)
        for g in range(groups):
            part = jnp.dot(
                pairs[g],
                wout[pl.ds(g * wout_rows, wout_rows), span],
                preferred_element_type=F32,
            )
            acc = acc + part.astype(BF16).astype(F32)
        out_ref[:, span] = acc.astype(BF16)

    tok_gather.drain()
    wout_gather.drain()
    for j, remote in exchanged:

        @pl.when(j != y)
        def _():
            remote.wait_send()

    @pl.when(c == 0)
    def _():
        for s in range(subs):
            chunk_wait(s, own_ss.at[s])

    @pl.loop(1, k_up + 1)
    def _(k):
        for d in range(2):
            for s in range(subs):
                more = jnp.logical_not(sends(d, k + 1, s))

                @pl.when(jnp.logical_and(sends(d, k, s), more))
                def _():
                    chunk_wait(s, ring_ss.at[d, s])

                more = jnp.logical_not(needs(d, k + 1, s))

                @pl.when(jnp.logical_and(needs(d, k, s), more))
                def _():
                    chunk_wait(s, d2d_ss.at[d, s])

    stays = owner_core == c
    pieces = att_send.shape[0]

    @pl.when(stays)
    def _():
        sent = att_send.at[pl.ds(0, pieces - 1)]
        pltpu.make_async_copy(sent, sent, att_ss).wait()

    @pl.when(jnp.logical_not(stays))
    def _():
        pltpu.make_async_copy(att_send, att_send, att_ss).wait()


def on_device(
    nz,
    tokens,
    query_weight,
    key_weight,
    value_weight,
    query_gain,
    key_gain,
    log_gate_total,
    output_weight,
):
    rows_tp, depth = tokens.shape
    width = query_weight.shape[1]
    blk, heads = log_gate_total.shape
    half = 2 * blk
    k_up = nz // 2
    dma = pltpu.SemaphoreType.DMA
    any_spec = pl.BlockSpec(memory_space=pl.ANY)
    vmem_spec = pl.BlockSpec(memory_space=pltpu.VMEM)
    return pl.pallas_call(
        functools.partial(kernel, nz),
        out_shape=jax.ShapeDtypeStruct((rows_tp, output_weight.shape[1]), BF16),
        in_specs=[any_spec] * 8,
        out_specs=vmem_spec,
        scratch_shapes=[
            pltpu.VMEM((blk, depth), BF16),
            pltpu.VMEM((depth, 3 * width), BF16),
            pltpu.VMEM((NX * NC * output_weight.shape[0], output_weight.shape[1]), BF16),
            pltpu.VMEM((blk, 2 * width), F32),
            pltpu.VMEM((2, blk, LANES), BF16),
            pltpu.VMEM((2, blk // 2, LANES), BF16),
            pltpu.VMEM((2, 1, HEAD), F32),
            pltpu.VMEM((heads, blk), F32),
            pltpu.VMEM((2, 8, LANES), F32),
            pltpu.VMEM((2, blk // 2, LANES), BF16),
            pltpu.VMEM((2, 8, LANES), F32),
            pltpu.VMEM((nz, 2, 2, blk, LANES), BF16),
            pltpu.VMEM((nz, 2, 8, LANES), F32),
            pltpu.VMEM((half, LANES), BF16),
            pltpu.VMEM((half, LANES), F32),
            pltpu.VMEM((half, LANES), F32),
            pltpu.VMEM((half, LANES), F32),
            pltpu.VMEM((2 * half, LANES), BF16),
            pltpu.VMEM((2 * NX * NC, rows_tp // 2, LANES), BF16),
            pltpu.VMEM((NX * NY, rows_tp // 2, LANES), BF16),
            dma((8,)),
            dma,
            dma((13,)),
            dma,
            dma((13,)),
            dma((3, 2)),
            dma((3, 2)),
            dma((2, 2)),
            dma((2, k_up, 2)),
            dma((2, 2)),
            dma((2, k_up, 2)),
            dma((2,)),
            dma((2,)),
            dma,
            dma,
        ],
        compiler_params=pltpu.CompilerParams(
            collective_id=0, has_side_effects=True, vmem_limit_bytes=60 * 1024 * 1024
        ),
    )(
        tokens,
        query_weight,
        key_weight,
        value_weight,
        query_gain[None, :],
        key_gain[None, :],
        log_gate_total.T,
        output_weight,
    )


def solution(mesh):
    placed = (
        P(("sp", "tp"), None),
        P(None, "tp"),
        P(None, "tp"),
        P(None, "tp"),
        P(),
        P(),
        P("sp", "tp"),
        P("tp", None),
    )
    nz = mesh.shape["sp"] // NY
    return jax.shard_map(
        functools.partial(on_device, nz),
        mesh=mesh,
        in_specs=placed,
        out_specs=P(("sp", "tp"), None),
        check_vma=False,
    )
```

time: 79.6 us -> 73.3 us (0.921)
  the two profiles are of different devices: /device:TPU:385 before, /device:TPU:353 now
where the time goes in v3:
time: 73.3 us; the launch traced here: 73.1 us
  Pallas kernels  71.5 us (98%)
  local copies, waits for them, and re-layouts  1.62 us (2%)
    pallas_call x1, Pallas kernels, on_device(): pl.pallas_call(functools.partial(kernel, nz), out_shape=jax.ShapeDtypeStr...  71.5 us
    unnamed x1, local copies, waits for them, and re-layouts  1.62 us

profile of v3, /device:TPU:353, one launch (start us, length us, event | category | flops | bytes accessed | tf_op | source)
XLA Modules:
  0.0 73.1 jit_solution(10689431721137373003)
XLA Ops:
  0.0 71.5 %shard_map.82 = bf16[48,2048]{1,0:T(8,128)(2,1)} custom-call(bf16[48,2048]{1,0:T(8,128)(2,1)} %tokens_ref.1, bf16[2048,128]{1,0:T(8,128)(2,1)} %wq_ref.1, bf16[2048,128]{1,0:T(8,128)(2,1)} %wk_ref.1, bf16[2048,128]{1,0:T(8,128)(2,1)} %wv_ref.1, f32[1,64]{1,0:T(1,128)} %bitcast.4, f32[1,64]{1,0:T(1,128)} %bitcast.5, f32[2,384]{1,0:T(2,128)} %bitcast.3, ...), custom_call_target="tpu_custom_call" | custom-call | tf_op jit(solution)/shard_map/pallas_call | solution.py:637
  71.5 1.6 %copy.10 = bf16[48,2048]{1,0:T(8,128)(2,1)} copy(bf16[48,2048]{1,0:T(8,128)(2,1)} %shard_map.82) | data formatting | bytes 393216

commit v4 on v3

--- a/solution.py
+++ b/solution.py
@@ -66,23 +66,30 @@
         self.send(-1, 0, 7)
         self.send(1, 1, 8)
 
-    def finish_links(self):
+    def relay_near(self):
         self.arrive(-1, self.c, 1, 1)
         self.send(-1, 1, 9)
         self.arrive(1, self.c, 0, 4)
         self.send(1, 0, 10)
+
+    def relay_far(self):
         self.arrive(-2, self.c, 0, 2)
         self.send(-2, 0, 11)
         self.arrive(2, self.c, 1, 5)
         self.send(2, 1, 12)
 
-    def finish(self):
+    def finish_own(self):
+        self.arrive(0, 1 - self.c, None, 6)
+
+    def finish_near(self):
         other = 1 - self.c
-        self.arrive(0, other, None, 6)
         self.arrive(-1, other, 0, 7)
         self.arrive(1, other, 1, 8)
         self.arrive(-1, other, 1, 9)
         self.arrive(1, other, 0, 10)
+
+    def finish_far(self):
+        other = 1 - self.c
         self.arrive(-2, other, 0, 11)
         self.arrive(2, other, 1, 12)
 
@@ -105,7 +112,7 @@
     tok,
     wqkv,
     wout,
-    raw,
+    q_raw,
     kv_send,
     q_send,
     gain_v,
@@ -122,6 +129,7 @@
     v_s,
     att_send,
     att_recv,
+    acc_s,
     lsem,
     tok_ss,
     tok_rs,
@@ -237,56 +245,73 @@
         def _():
             pltpu.make_async_copy(src, dst, a2a_rs.at[n, par]).start()
 
-        exchanged.append((j, remote))
 
     def received(n, s, dst):
         pltpu.make_async_copy(dst, dst, a2a_rs.at[n, s]).wait()
 
-    exchanged = []
     for i in range(2):
         exchange(2, i, gate_send.at[i], gate_recv.at[par])
 
+    lane = lax.broadcasted_iota(jnp.int32, (LANES, LANES), 1)
+    low = lane < HEAD
+    qgain, kgain = [jnp.concatenate([gain_v[i], gain_v[i]], axis=1) for i in range(2)]
+    chip_rows = NC * rows_tp
+
+    def head_norm(raw_part, gain):
+        low_part = low[: raw_part.shape[0]]
+        square = raw_part * raw_part
+        lo = jnp.sum(jnp.where(low_part, square, 0.0), axis=1, keepdims=True) * (1.0 / HEAD)
+        hi = jnp.sum(jnp.where(low_part, 0.0, square), axis=1, keepdims=True) * (1.0 / HEAD)
+        inverse = jnp.where(low_part, lax.rsqrt(lo + NORM_EPS), lax.rsqrt(hi + NORM_EPS))
+        return raw_part * inverse * gain
+
+    def rows_of(dx):
+        slot = lax.rem(x + dx + NX, NX)
+        return pl.ds(pl.multiple_of(slot * chip_rows, chip_rows), chip_rows)
+
+    def project_keys(dx):
+        rows = rows_of(dx)
+        low_part = low[:chip_rows]
+        raw = jnp.dot(tok[rows, :], wqkv[:, width : 3 * width], preferred_element_type=F32)
+        k_part = head_norm(raw[:, 0:width], kgain)
+        v_part = raw[:, width : 2 * width]
+        k_roll = pltpu.roll(k_part, HEAD, 1)
+        v_roll = pltpu.roll(v_part, HEAD, 1)
+        kv_send[0, rows, :] = jnp.where(low_part, k_part, v_roll).astype(BF16)
+        kv_send[1, rows, :] = jnp.where(low_part, k_roll, v_part).astype(BF16)
+        for i in range(2):
+            exchange(0, i, kv_send.at[i, rows], kv_all.at[z, par, owner_core, rows])
+
+    def project_queries(dx):
+        rows = rows_of(dx)
+        raw = jnp.dot(tok[rows, :], wqkv[:, 0:width], preferred_element_type=F32)
+        q_raw[rows, :] = head_norm(raw, qgain) * (HEAD**-0.5)
+
+    for load in loads:
+        load.wait()
+    tok_gather.finish_own()
+    project_keys(0)
     tok_gather.relay()
-    tok_gather.finish_links()
+    project_queries(0)
+    tok_gather.relay_near()
+    tok_gather.finish_near()
+    project_keys(1)
+    project_keys(-1)
+    tok_gather.relay_far()
     load_wout.wait()
     wout_gather = RowGather(wout, wout_rows, x, c, (right, left, partner), wo_ss, wo_rs)
     wout_gather.start()
-    for load in loads:
-        load.wait()
-    tok_gather.finish()
-
-    lane = lax.broadcasted_iota(jnp.int32, (LANES, LANES), 1)
-    low = lane < HEAD
-    qgain, kgain = [jnp.concatenate([gain_v[i], gain_v[i]], axis=1) for i in range(2)]
-
-    def head_norm(raw_part, gain):
-        square = raw_part * raw_part
-        lo = jnp.sum(jnp.where(low, square, 0.0), axis=1, keepdims=True) * (1.0 / HEAD)
-        hi = jnp.sum(jnp.where(low, 0.0, square), axis=1, keepdims=True) * (1.0 / HEAD)
-        inverse = jnp.where(low, lax.rsqrt(lo + NORM_EPS), lax.rsqrt(hi + NORM_EPS))
-        return raw_part * inverse * gain
-
-    raw[...] = jnp.dot(tok[...], wqkv[:, width : 3 * width], preferred_element_type=F32)
-    for t in range(tiles_blk):
-        rows = pl.ds(t * LANES, LANES)
-        k_part = head_norm(raw[rows, 0:width], kgain)
-        v_part = raw[rows, width : 2 * width]
-        k_roll = pltpu.roll(k_part, HEAD, 1)
-        v_roll = pltpu.roll(v_part, HEAD, 1)
-        kv_send[0, rows, :] = jnp.where(low, k_part, v_roll).astype(BF16)
-        kv_send[1, rows, :] = jnp.where(low, k_roll, v_part).astype(BF16)
-    for i in range(2):
-        exchange(0, i, kv_send.at[i], kv_all.at[z, par, owner_core])
-
-    raw[:, 0:width] = jnp.dot(tok[...], wqkv[:, 0:width], preferred_element_type=F32)
-    for t in range(tiles_blk):
-        rows = pl.ds(t * LANES, LANES)
-        raw[rows, width : 2 * width] = head_norm(raw[rows, 0:width], qgain) * (HEAD**-0.5)
+    project_queries(1)
+    tok_gather.finish_far()
+    project_keys(2)
+
+    project_queries(-1)
+    project_queries(2)
     pack = blk // 2
     step = 64
     for t in range(pack // step):
-        first = raw[pl.ds(t * step, step), width : 2 * width]
-        second = raw[pl.ds(pack + t * step, step), width : 2 * width]
+        first = q_raw[pl.ds(t * step, step), :]
+        second = q_raw[pl.ds(pack + t * step, step), :]
         rows = pl.ds(t * step, step)
         q_send[0, rows, :] = jnp.where(low[:step], first, pltpu.roll(second, HEAD, 1)).astype(BF16)
         q_send[1, rows, :] = jnp.where(low[:step], pltpu.roll(first, HEAD, 1), second).astype(BF16)
@@ -501,7 +526,8 @@
 
         @pl.when(k == 5)
         def _():
-            wout_gather.finish_links()
+            wout_gather.relay_near()
+            wout_gather.relay_far()
 
     for s in range(subs):
         pass_on(s, k_up, s)
@@ -533,11 +559,11 @@
                 src_ref=src,
                 dst_ref=att_recv.at[head],
                 send_sem=att_ss,
-                recv_sem=att_rs,
+                recv_sem=att_rs.at[x],
                 device_id=(z * NY + ty, t),
                 device_id_type=MESH,
             )
-            local = pltpu.make_async_copy(src, att_recv.at[head], att_rs)
+            local = pltpu.make_async_copy(src, att_recv.at[head], att_rs.at[x])
             is_self = jnp.logical_and(ty == y, tp == t)
 
             @pl.when(jnp.logical_not(is_self))
@@ -548,38 +574,45 @@
             def _():
                 local.start()
 
-    wout_gather.finish()
-    pltpu.make_async_copy(att_recv, att_recv, att_rs).wait()
-
-    groups = NX * NC
-    pairs = []
-    for g in range(groups):
-        even, odd = [att_recv[2 * g + n].astype(F32) for n in range(2)]
-        early = jnp.where(low[:few], even, pltpu.roll(odd, HEAD, 1))
-        late = jnp.where(low[:few], pltpu.roll(even, HEAD, 1), odd)
-        pairs.append(jnp.concatenate([early, late], axis=0).astype(BF16))
+    wout_gather.finish_own()
+    wout_gather.finish_near()
+    wout_gather.finish_far()
     cols = 256
-
-    @pl.loop(0, out_ref.shape[1] // cols)
-    def _(t):
-        span = pl.ds(pl.multiple_of(t * cols, cols), cols)
-        acc = jnp.zeros((rows_tp, cols), F32)
-        for g in range(groups):
-            part = jnp.dot(
-                pairs[g],
-                wout[pl.ds(g * wout_rows, wout_rows), span],
-                preferred_element_type=F32,
-            )
-            acc = acc + part.astype(BF16).astype(F32)
-        out_ref[:, span] = acc.astype(BF16)
+    for n, dx in enumerate((0, 1, -1, 2)):
+        slot = lax.rem(x + dx + NX, NX)
+        heads = att_recv.at[pl.ds(slot * NY, NY)]
+        pltpu.make_async_copy(heads, heads, att_rs.at[slot]).wait()
+        pairs = []
+        for g in range(NC):
+            even, odd = [att_recv[slot * NY + 2 * g + i].astype(F32) for i in range(2)]
+            early = jnp.where(low[:few], even, pltpu.roll(odd, HEAD, 1))
+            late = jnp.where(low[:few], pltpu.roll(even, HEAD, 1), odd)
+            pairs.append(jnp.concatenate([early, late], axis=0).astype(BF16))
+
+        @pl.loop(0, out_ref.shape[1] // cols)
+        def _(t):
+            span = pl.ds(pl.multiple_of(t * cols, cols), cols)
+            acc = None if n == 0 else acc_s[:, span]
+            for g in range(NC):
+                first = pl.multiple_of((slot * NC + g) * wout_rows, wout_rows)
+                part = jnp.dot(
+                    pairs[g], wout[pl.ds(first, wout_rows), span], preferred_element_type=F32
+                )
+                part = part.astype(BF16).astype(F32)
+                acc = part if acc is None else acc + part
+            if n < NX - 1:
+                acc_s[:, span] = acc
+            else:
+                out_ref[:, span] = acc.astype(BF16)
 
     tok_gather.drain()
     wout_gather.drain()
-    for j, remote in exchanged:
-
-        @pl.when(j != y)
-        def _():
-            remote.wait_send()
+    for i in range(2):
+
+        @pl.when(2 * c + i != y)
+        def _():
+            for n, sent in enumerate((kv_send.at[i], q_send.at[i], gate_send.at[i])):
+                pltpu.make_async_copy(sent, sent, a2a_ss.at[n, i]).wait()
 
     @pl.when(c == 0)
     def _():
@@ -636,14 +669,14 @@
     vmem_spec = pl.BlockSpec(memory_space=pltpu.VMEM)
     return pl.pallas_call(
         functools.partial(kernel, nz),
-        out_shape=jax.ShapeDtypeStruct((rows_tp, output_weight.shape[1]), BF16),
+        out_shape=pltpu.VMEM((rows_tp, output_weight.shape[1]), BF16),
         in_specs=[any_spec] * 8,
         out_specs=vmem_spec,
         scratch_shapes=[
             pltpu.VMEM((blk, depth), BF16),
             pltpu.VMEM((depth, 3 * width), BF16),
             pltpu.VMEM((NX * NC * output_weight.shape[0], output_weight.shape[1]), BF16),
-            pltpu.VMEM((blk, 2 * width), F32),
+            pltpu.VMEM((blk, width), F32),
             pltpu.VMEM((2, blk, LANES), BF16),
             pltpu.VMEM((2, blk // 2, LANES), BF16),
             pltpu.VMEM((2, 1, HEAD), F32),
@@ -660,6 +693,7 @@
             pltpu.VMEM((2 * half, LANES), BF16),
             pltpu.VMEM((2 * NX * NC, rows_tp // 2, LANES), BF16),
             pltpu.VMEM((NX * NY, rows_tp // 2, LANES), BF16),
+            pltpu.VMEM((rows_tp, output_weight.shape[1]), F32),
             dma((8,)),
             dma,
             dma((13,)),
@@ -674,7 +708,7 @@
             dma((2,)),
             dma((2,)),
             dma,
-            dma,
+            dma((NX,)),
         ],
         compiler_params=pltpu.CompilerParams(
             collective_id=0, has_side_effects=True, vmem_limit_bytes=60 * 1024 * 1024

time: 73.3 us -> 71.3 us (0.973)
  Pallas kernels: 71.5 us -> 70.5 us
  local copies, waits for them, and re-layouts: 1.62 us -> 0.68 us
    pallas_call x1, Pallas kernels: 71.5 us -> 70.5 us  [on_device(): pl.pallas_call(functools.partial(kernel, nz), out_shape=pltpu.VMEM((rows_...]
    unnamed x1, local copies, waits for them, and re-layouts: 1.62 us -> 0.68 us
where the time goes in v4:
time: 71.3 us; the launch traced here: 71.2 us
  Pallas kernels  70.5 us (99%)
    pallas_call x1, Pallas kernels, on_device(): pl.pallas_call(functools.partial(kernel, nz), out_shape=pltpu.VMEM((rows_...  70.5 us

profile of v4, /device:TPU:353, one launch (start us, length us, event | category | flops | bytes accessed | tf_op | source)
XLA Modules:
  0.0 71.2 jit_solution(1704675965168384767)
XLA Ops:
  0.0 70.5 %shard_map.82 = bf16[48,2048]{1,0:T(8,128)(2,1)S(1)} custom-call(bf16[48,2048]{1,0:T(8,128)(2,1)} %tokens_ref.1, bf16[2048,128]{1,0:T(8,128)(2,1)} %wq_ref.1, bf16[2048,128]{1,0:T(8,128)(2,1)} %wk_ref.1, bf16[2048,128]{1,0:T(8,128)(2,1)} %wv_ref.1, f32[1,64]{1,0:T(1,128)} %bitcast.4, f32[1,64]{1,0:T(1,128)} %bitcast.5, f32[2,384]{1,0:T(2,128)} %bitcast.3, ...), custom_call_target="tpu_custom_call" | custom-call | tf_op jit(solution)/shard_map/pallas_call | solution.py:670
  70.5 0.7 copy.10

commit v5 on v4

--- a/solution.py
+++ b/solution.py
@@ -216,22 +216,34 @@
     par = lax.rem(y, 2)
     tiles_blk = blk // LANES
 
+    chip_rows = NC * rows_tp
+    part_rows = blk // 2
     for small in smalls:
         small.wait()
     sublane = lax.broadcasted_iota(jnp.int32, (8, LANES), 0)
+    wide_lane = lax.broadcasted_iota(jnp.int32, (8, half), 1)
     for i in range(2):
+        line = jnp.broadcast_to(gate_v[i : i + 1, :], (8, blk))
+        turned = line
+        for n in range(1, NX):
+            turned = jnp.where(x == n, pltpu.roll(line, blk - n * chip_rows, 1), turned)
+        line = jnp.concatenate([turned, jnp.zeros((8, half - blk), F32)], axis=1)
+        moved = pltpu.roll(line, part_rows, 1)
+        first = jnp.where(wide_lane < part_rows, line, 0.0)
+        second = jnp.where(wide_lane >= blk, moved, 0.0)
+        line = first + second
+        line = jnp.where(par == 0, line, pltpu.roll(line, part_rows, 1))
         tile = jnp.zeros((8, LANES), F32)
-        for t in range(tiles_blk):
-            row = jnp.broadcast_to(gate_v[i : i + 1, t * LANES : (t + 1) * LANES], (8, LANES))
-            tile = jnp.where(sublane == par * tiles_blk + t, row, tile)
+        for t in range(2 * tiles_blk):
+            tile = jnp.where(sublane == t, line[:, t * LANES : (t + 1) * LANES], tile)
         gate_send[i] = tile
 
-    def exchange(n, i, src, dst):
+    def exchange(n, kind, i, src, dst):
         j = 2 * c + i
         remote = pltpu.make_async_remote_copy(
             src_ref=src,
             dst_ref=dst,
-            send_sem=a2a_ss.at[n, i],
+            send_sem=a2a_ss.at[kind, i],
             recv_sem=a2a_rs.at[n, par],
             device_id=device(z, j, x, owner_core),
             device_id_type=MESH,
@@ -245,18 +257,15 @@
         def _():
             pltpu.make_async_copy(src, dst, a2a_rs.at[n, par]).start()
 
-
     def received(n, s, dst):
         pltpu.make_async_copy(dst, dst, a2a_rs.at[n, s]).wait()
 
     for i in range(2):
-        exchange(2, i, gate_send.at[i], gate_recv.at[par])
+        exchange(3, 2, i, gate_send.at[i], gate_recv.at[par])
 
     lane = lax.broadcasted_iota(jnp.int32, (LANES, LANES), 1)
     low = lane < HEAD
     qgain, kgain = [jnp.concatenate([gain_v[i], gain_v[i]], axis=1) for i in range(2)]
-    chip_rows = NC * rows_tp
-
     def head_norm(raw_part, gain):
         low_part = low[: raw_part.shape[0]]
         square = raw_part * raw_part
@@ -270,22 +279,26 @@
         return pl.ds(pl.multiple_of(slot * chip_rows, chip_rows), chip_rows)
 
     def project_keys(dx):
-        rows = rows_of(dx)
+        place = dx % NX
+        kept = pl.ds(place * chip_rows, chip_rows)
         low_part = low[:chip_rows]
-        raw = jnp.dot(tok[rows, :], wqkv[:, width : 3 * width], preferred_element_type=F32)
+        raw = jnp.dot(tok[rows_of(dx), :], wqkv[:, width : 3 * width], preferred_element_type=F32)
         k_part = head_norm(raw[:, 0:width], kgain)
         v_part = raw[:, width : 2 * width]
         k_roll = pltpu.roll(k_part, HEAD, 1)
         v_roll = pltpu.roll(v_part, HEAD, 1)
-        kv_send[0, rows, :] = jnp.where(low_part, k_part, v_roll).astype(BF16)
-        kv_send[1, rows, :] = jnp.where(low_part, k_roll, v_part).astype(BF16)
+        kv_send[0, kept, :] = jnp.where(low_part, k_part, v_roll).astype(BF16)
+        kv_send[1, kept, :] = jnp.where(low_part, k_roll, v_part).astype(BF16)
+        chunk = place // 2
+        first = pl.multiple_of(par * part_rows + (place % 2) * chip_rows, chip_rows)
+        there = kv_all.at[z, chunk, owner_core, pl.ds(first, chip_rows)]
         for i in range(2):
-            exchange(0, i, kv_send.at[i, rows], kv_all.at[z, par, owner_core, rows])
+            exchange(chunk, 0, i, kv_send.at[i, kept], there)
 
     def project_queries(dx):
-        rows = rows_of(dx)
-        raw = jnp.dot(tok[rows, :], wqkv[:, 0:width], preferred_element_type=F32)
-        q_raw[rows, :] = head_norm(raw, qgain) * (HEAD**-0.5)
+        raw = jnp.dot(tok[rows_of(dx), :], wqkv[:, 0:width], preferred_element_type=F32)
+        kept = pl.ds((dx % NX) * chip_rows, chip_rows)
+        q_raw[kept, :] = head_norm(raw, qgain) * (HEAD**-0.5)
 
     for load in loads:
         load.wait()
@@ -305,19 +318,6 @@
     tok_gather.finish_far()
     project_keys(2)
 
-    project_queries(-1)
-    project_queries(2)
-    pack = blk // 2
-    step = 64
-    for t in range(pack // step):
-        first = q_raw[pl.ds(t * step, step), :]
-        second = q_raw[pl.ds(pack + t * step, step), :]
-        rows = pl.ds(t * step, step)
-        q_send[0, rows, :] = jnp.where(low[:step], first, pltpu.roll(second, HEAD, 1)).astype(BF16)
-        q_send[1, rows, :] = jnp.where(low[:step], pltpu.roll(first, HEAD, 1), second).astype(BF16)
-    for i in range(2):
-        exchange(1, i, q_send.at[i], q_recv.at[par])
-
     subs = 2
 
     def chunk_copies(b, s, target, send_sem, recv_sem):
@@ -368,16 +368,34 @@
         return jnp.logical_and(receives(1, k, s), block_of(1, k) < z)
 
     for s in range(subs):
-        received(2, s, gate_recv.at[s])
+        received(3, s, gate_recv.at[s])
     gate_all[z, c] = gate_recv[0] + gate_recv[1]
-    for s in range(subs):
-        received(0, s, kv_all.at[z, s, c])
+    def own_to_ring(s):
+        for n in range(2):
+            received(s, n, kv_all.at[z, s, c, pl.ds(n * part_rows, part_rows)])
         for d in range(2):
 
             @pl.when(sends(d, 1, s))
             def _():
                 for copy in chunk_copies(z, s, links[d], ring_ss.at[d, s], ring_rs.at[d, 0, s]):
                     copy.start()
+
+    own_to_ring(0)
+
+    project_queries(-1)
+    project_queries(2)
+    pack = blk // 2
+    step = 64
+    for t in range(pack // step):
+        first = q_raw[pl.ds(t * step, step), :]
+        second = q_raw[pl.ds(pack + t * step, step), :]
+        rows = pl.ds(t * step, step)
+        q_send[0, rows, :] = jnp.where(low[:step], first, pltpu.roll(second, HEAD, 1)).astype(BF16)
+        q_send[1, rows, :] = jnp.where(low[:step], pltpu.roll(first, HEAD, 1), second).astype(BF16)
+    for i in range(2):
+        exchange(2, 1, i, q_send.at[i], q_recv.at[par])
+
+    own_to_ring(1)
 
     @pl.when(c == 0)
     def _():
@@ -392,18 +410,28 @@
     m_s[...] = jnp.full(m_s.shape, -1e30, F32)
     o_s[...] = jnp.zeros(o_s.shape, F32)
     for s in range(subs):
-        received(1, s, q_recv.at[s])
+        received(2, s, q_recv.at[s])
         for t in range(pack // step):
             packed = q_recv[s, pl.ds(t * step, step), :].astype(F32)
             second = pltpu.roll(packed, HEAD, 1)
             for n, rows in enumerate((packed, second)):
-                first_row = s * blk + n * pack + t * step
+                first_row = n * blk + s * part_rows + t * step
                 q_s[pl.ds(first_row, step), :] = jnp.where(low[:step], rows, 0.0).astype(BF16)
 
     lane_row = lax.broadcasted_iota(jnp.int32, (1, LANES), 1)
     ones_low = jnp.where(lane_row < HEAD, 1.0, 0.0).astype(BF16)
     keep_high = jnp.where(lane_row < HEAD, 0.0, 1.0).astype(BF16)
     tiles = half // QT
+
+    def position(row):
+        late = (row >= blk).astype(jnp.int32)
+        row = row - late * blk
+        odd_y = (row >= part_rows).astype(jnp.int32)
+        row = row - odd_y * part_rows
+        next_slot = (row >= chip_rows).astype(jnp.int32)
+        row = row - next_slot * chip_rows
+        slot = lax.bitwise_and(2 * late + next_slot + x, NX - 1)
+        return odd_y * blk + slot * chip_rows + row
 
     def update(pieces, masked=False):
         count = len(pieces) * blk
@@ -430,11 +458,9 @@
             )
             score = score - gate_row
             if masked:
-                shape = score.shape
-                row_id = lax.broadcasted_iota(jnp.int32, shape, 0) + t * QT
-                score = jnp.where(
-                    lax.broadcasted_iota(jnp.int32, shape, 1) <= row_id, score, -jnp.inf
-                )
+                query_pos = position(lax.broadcasted_iota(jnp.int32, (QT, 1), 0) + t * QT)
+                key_pos = position(lax.broadcasted_iota(jnp.int32, (1, count), 1))
+                score = jnp.where(key_pos <= query_pos, score, -jnp.inf)
             return score
 
         def add(t, score):
@@ -455,6 +481,52 @@
             add(t, score)
             score = following
 
+    def pieces_of(d, k, s):
+        return [(block_of(d, k), s, core) for core in range(2)]
+
+    def relayed(d, k, s):
+        chunk_wait(s, d2d_rs.at[d, k - 1, s])
+
+    def pair(k, s):
+        @pl.when(needs(1, k, s))
+        def _():
+            relayed(0, k, s)
+            relayed(1, k, s)
+            update(pieces_of(0, k, s) + pieces_of(1, k, s))
+
+        @pl.when(jnp.logical_and(needs(0, k, s), jnp.logical_not(needs(1, k, s))))
+        def _():
+            relayed(0, k, s)
+            update(pieces_of(0, k, s))
+
+    def pass_on(d, k, s):
+        @pl.when(receives(d, k, s))
+        def _():
+            b = block_of(d, k)
+            chunk_wait(s, ring_rs.at[d, k - 1, s])
+
+            @pl.when(sends(d, k + 1, s))
+            def _():
+                @pl.when(sends(d, k, s))
+                def _():
+                    chunk_wait(s, ring_ss.at[d, s])
+
+                for copy in chunk_copies(b, s, links[d], ring_ss.at[d, s], ring_rs.at[d, k, s]):
+                    copy.start()
+
+            @pl.when(needs(d, k, s))
+            def _():
+                @pl.when(jnp.logical_and(k > 1, needs(d, k - 1, s)))
+                def _():
+                    chunk_wait(s, d2d_ss.at[d, s])
+
+                for copy in chunk_copies(
+                    b, s, partner, d2d_ss.at[d, s], d2d_rs.at[d, k - 1, s]
+                ):
+                    copy.start()
+
+    pass_on(0, 1, 0)
+    pass_on(1, 1, 0)
     update([(z, s, c) for s in range(subs)], masked=True)
 
     @pl.when(c == 1)
@@ -463,57 +535,12 @@
             chunk_wait(s, own_rs.at[s])
         update([(z, s, 0) for s in range(subs)])
 
-    def pieces_of(d, k, s):
-        return [(block_of(d, k), s, core) for core in range(2)]
-
-    def relayed(d, k, s):
-        chunk_wait(s, d2d_rs.at[d, k - 1, s])
-
-    def pair(k, s):
-        @pl.when(needs(1, k, s))
-        def _():
-            relayed(0, k, s)
-            relayed(1, k, s)
-            update(pieces_of(0, k, s) + pieces_of(1, k, s))
-
-        @pl.when(jnp.logical_and(needs(0, k, s), jnp.logical_not(needs(1, k, s))))
-        def _():
-            relayed(0, k, s)
-            update(pieces_of(0, k, s))
-
-    def pass_on(d, k, s):
-        @pl.when(receives(d, k, s))
-        def _():
-            b = block_of(d, k)
-            chunk_wait(s, ring_rs.at[d, k - 1, s])
-
-            @pl.when(sends(d, k + 1, s))
-            def _():
-                @pl.when(sends(d, k, s))
-                def _():
-                    chunk_wait(s, ring_ss.at[d, s])
-
-                for copy in chunk_copies(b, s, links[d], ring_ss.at[d, s], ring_rs.at[d, k, s]):
-                    copy.start()
-
-            @pl.when(needs(d, k, s))
-            def _():
-                @pl.when(jnp.logical_and(k > 1, needs(d, k - 1, s)))
-                def _():
-                    chunk_wait(s, d2d_ss.at[d, s])
-
-                for copy in chunk_copies(
-                    b, s, partner, d2d_ss.at[d, s], d2d_rs.at[d, k - 1, s]
-                ):
-                    copy.start()
-
     @pl.loop(1, k_up)
     def _(k):
-        pass_on(0, k, 0)
-        pass_on(1, k, 0)
-
         @pl.when(k > 1)
         def _():
+            pass_on(0, k, 0)
+            pass_on(1, k, 0)
             pair(k - 1, 1)
 
         pass_on(0, k, 1)
@@ -551,10 +578,13 @@
 
     head = NY * x + y
     att = []
-    for s in range(subs):
-        for t in range(NX * NC):
-            ty = 2 * c + s
-            src = att_send.at[s * NX * NC + t]
+    for place in range(NX):
+        for n in range(2 * NC):
+            odd_y, core = n // NC, n % NC
+            ty = 2 * c + odd_y
+            t = lax.rem(x + place, NX) * NC + core
+            piece = (place // 2) * NX * NC + odd_y * NX + (place % 2) * NC + core
+            src = att_send.at[piece]
             remote = pltpu.make_async_remote_copy(
                 src_ref=src,
                 dst_ref=att_recv.at[head],
@@ -589,9 +619,8 @@
             late = jnp.where(low[:few], pltpu.roll(even, HEAD, 1), odd)
             pairs.append(jnp.concatenate([early, late], axis=0).astype(BF16))
 
-        @pl.loop(0, out_ref.shape[1] // cols)
-        def _(t):
-            span = pl.ds(pl.multiple_of(t * cols, cols), cols)
+        for t in range(out_ref.shape[1] // cols):
+            span = pl.ds(t * cols, cols)
             acc = None if n == 0 else acc_s[:, span]
             for g in range(NC):
                 first = pl.multiple_of((slot * NC + g) * wout_rows, wout_rows)
@@ -700,7 +729,7 @@
             dma,
             dma((13,)),
             dma((3, 2)),
-            dma((3, 2)),
+            dma((4, 2)),
             dma((2, 2)),
             dma((2, k_up, 2)),
             dma((2, 2)),

time: 71.3 us -> 66.6 us (0.934)
  Pallas kernels: 70.5 us -> 65.8 us
    pallas_call x1, Pallas kernels: 70.5 us -> 65.8 us  [on_device(): pl.pallas_call(functools.partial(kernel, nz), out_shape=pltpu.VMEM((rows_...]
where the time goes in v5:
time: 66.6 us; the launch traced here: 66.5 us
  Pallas kernels  65.8 us (99%)
  local copies, waits for them, and re-layouts  0.68 us (1%)
    pallas_call x1, Pallas kernels, on_device(): pl.pallas_call(functools.partial(kernel, nz), out_shape=pltpu.VMEM((rows_...  65.8 us

profile of v5, /device:TPU:353, one launch (start us, length us, event | category | flops | bytes accessed | tf_op | source)
XLA Modules:
  0.0 66.5 jit_solution(16855046536417831646)
XLA Ops:
  0.0 65.8 %shard_map.82 = bf16[48,2048]{1,0:T(8,128)(2,1)S(1)} custom-call(bf16[48,2048]{1,0:T(8,128)(2,1)} %tokens_ref.1, bf16[2048,128]{1,0:T(8,128)(2,1)} %wq_ref.1, bf16[2048,128]{1,0:T(8,128)(2,1)} %wk_ref.1, bf16[2048,128]{1,0:T(8,128)(2,1)} %wv_ref.1, f32[1,64]{1,0:T(1,128)} %bitcast.4, f32[1,64]{1,0:T(1,128)} %bitcast.5, f32[2,384]{1,0:T(2,128)} %bitcast.3, ...), custom_call_target="tpu_custom_call" | custom-call | tf_op jit(solution)/shard_map/pallas_call | solution.py:699
  65.8 0.7 %copy.10 = bf16[48,2048]{1,0:T(8,128)(2,1)} copy(bf16[48,2048]{1,0:T(8,128)(2,1)S(1)} %shard_map.82) | data formatting | bytes 393216

commit v6 on v5

--- a/solution.py
+++ b/solution.py
@@ -67,10 +67,10 @@
         self.send(1, 1, 8)
 
     def relay_near(self):
+        self.arrive(1, self.c, 0, 4)
+        self.send(1, 0, 10)
         self.arrive(-1, self.c, 1, 1)
         self.send(-1, 1, 9)
-        self.arrive(1, self.c, 0, 4)
-        self.send(1, 0, 10)
 
     def relay_far(self):
         self.arrive(-2, self.c, 0, 2)
@@ -81,12 +81,15 @@
     def finish_own(self):
         self.arrive(0, 1 - self.c, None, 6)
 
-    def finish_near(self):
+    def finish_right(self):
+        other = 1 - self.c
+        self.arrive(1, other, 1, 8)
+        self.arrive(1, other, 0, 10)
+
+    def finish_left(self):
         other = 1 - self.c
         self.arrive(-1, other, 0, 7)
-        self.arrive(1, other, 1, 8)
         self.arrive(-1, other, 1, 9)
-        self.arrive(1, other, 0, 10)
 
     def finish_far(self):
         other = 1 - self.c
@@ -307,8 +310,9 @@
     tok_gather.relay()
     project_queries(0)
     tok_gather.relay_near()
-    tok_gather.finish_near()
+    tok_gather.finish_right()
     project_keys(1)
+    tok_gather.finish_left()
     project_keys(-1)
     tok_gather.relay_far()
     load_wout.wait()
@@ -334,9 +338,9 @@
             for piece in (pieces if s == 0 else pieces[:1])
         ]
 
-    def chunk_wait(s, sem):
+    def chunk_wait(s, sem, count=1):
         gate_rows = 8 * LANES * 4 // (LANES * 2)
-        sized = v_s.at[pl.ds(0, blk + gate_rows if s == 0 else blk)]
+        sized = v_s.at[pl.ds(0, count * (blk + gate_rows if s == 0 else blk))]
         pltpu.make_async_copy(sized, sized, sem).wait()
 
     k_up = nz // 2
@@ -421,7 +425,6 @@
     lane_row = lax.broadcasted_iota(jnp.int32, (1, LANES), 1)
     ones_low = jnp.where(lane_row < HEAD, 1.0, 0.0).astype(BF16)
     keep_high = jnp.where(lane_row < HEAD, 0.0, 1.0).astype(BF16)
-    tiles = half // QT
 
     def position(row):
         late = (row >= blk).astype(jnp.int32)
@@ -433,7 +436,7 @@
         slot = lax.bitwise_and(2 * late + next_slot + x, NX - 1)
         return odd_y * blk + slot * chip_rows + row
 
-    def update(pieces, masked=False):
+    def update(pieces, masked=False, order=tuple(range(half // QT)), between=None):
         count = len(pieces) * blk
 
         def keys():
@@ -475,28 +478,26 @@
             )
             m_s[rows, :] = m_new
 
-        score = score_of(0)
-        for t in range(tiles):
-            following = score_of(t + 1) if t + 1 < tiles else None
+        score = score_of(order[0])
+        for n, t in enumerate(order):
+            following = score_of(order[n + 1]) if n + 1 < len(order) else None
             add(t, score)
             score = following
+            if n == 0 and between is not None:
+                between()
 
     def pieces_of(d, k, s):
         return [(block_of(d, k), s, core) for core in range(2)]
 
-    def relayed(d, k, s):
-        chunk_wait(s, d2d_rs.at[d, k - 1, s])
-
     def pair(k, s):
         @pl.when(needs(1, k, s))
         def _():
-            relayed(0, k, s)
-            relayed(1, k, s)
+            chunk_wait(s, d2d_rs.at[k - 1, s], 2)
             update(pieces_of(0, k, s) + pieces_of(1, k, s))
 
         @pl.when(jnp.logical_and(needs(0, k, s), jnp.logical_not(needs(1, k, s))))
         def _():
-            relayed(0, k, s)
+            chunk_wait(s, d2d_rs.at[k - 1, s])
             update(pieces_of(0, k, s))
 
     def pass_on(d, k, s):
@@ -521,7 +522,7 @@
                     chunk_wait(s, d2d_ss.at[d, s])
 
                 for copy in chunk_copies(
-                    b, s, partner, d2d_ss.at[d, s], d2d_rs.at[d, k - 1, s]
+                    b, s, partner, d2d_ss.at[d, s], d2d_rs.at[k - 1, s]
                 ):
                     copy.start()
 
@@ -560,52 +561,88 @@
         pass_on(s, k_up, s)
     pair(k_up - 1, 1)
 
+    few = rows_tp // 2
+    head = NY * x + y
+
+    def send_attended(tile):
+        per_tile = QT // rows_tp
+        for n in range(tile * per_tile, (tile + 1) * per_tile):
+            first = o_s[pl.ds(n * rows_tp, few), :]
+            second = o_s[pl.ds(n * rows_tp + few, few), :]
+            first = pltpu.roll(first, HEAD, 1) / first
+            second = second / pltpu.roll(second, HEAD, 1)
+            att_send[n] = jnp.where(low[:few], first, second).astype(BF16)
+        for place in (2 * tile, 2 * tile + 1):
+            for n in range(2 * NC):
+                odd_y, core = n // NC, n % NC
+                ty = 2 * c + odd_y
+                t = lax.rem(x + place, NX) * NC + core
+                piece = (place // 2) * NX * NC + odd_y * NX + (place % 2) * NC + core
+                src = att_send.at[piece]
+                remote = pltpu.make_async_remote_copy(
+                    src_ref=src,
+                    dst_ref=att_recv.at[head],
+                    send_sem=att_ss,
+                    recv_sem=att_rs.at[x],
+                    device_id=(z * NY + ty, t),
+                    device_id_type=MESH,
+                )
+                local = pltpu.make_async_copy(src, att_recv.at[head], att_rs.at[x])
+                is_self = jnp.logical_and(ty == y, tp == t)
+
+                @pl.when(jnp.logical_not(is_self))
+                def _():
+                    remote.start()
+
+                @pl.when(is_self)
+                def _():
+                    local.start()
+
     @pl.when(z >= k_up)
     def _():
         for s in range(subs):
-            relayed(s, k_up, s)
-        update([(z - k_up, s, core) for s in range(subs) for core in range(2)])
-
-    odd_head = lax.rem(y, 2) == 1
-    few = rows_tp // 2
-
-    for n in range(half // rows_tp):
-        first = o_s[pl.ds(n * rows_tp, few), :]
-        second = o_s[pl.ds(n * rows_tp + few, few), :]
-        first = pltpu.roll(first, HEAD, 1) / first
-        second = second / pltpu.roll(second, HEAD, 1)
-        att_send[n] = jnp.where(low[:few], first, second).astype(BF16)
-
-    head = NY * x + y
-    att = []
-    for place in range(NX):
-        for n in range(2 * NC):
-            odd_y, core = n // NC, n % NC
-            ty = 2 * c + odd_y
-            t = lax.rem(x + place, NX) * NC + core
-            piece = (place // 2) * NX * NC + odd_y * NX + (place % 2) * NC + core
-            src = att_send.at[piece]
-            remote = pltpu.make_async_remote_copy(
-                src_ref=src,
-                dst_ref=att_recv.at[head],
-                send_sem=att_ss,
-                recv_sem=att_rs.at[x],
-                device_id=(z * NY + ty, t),
-                device_id_type=MESH,
-            )
-            local = pltpu.make_async_copy(src, att_recv.at[head], att_rs.at[x])
-            is_self = jnp.logical_and(ty == y, tp == t)
-
-            @pl.when(jnp.logical_not(is_self))
-            def _():
-                remote.start()
-
-            @pl.when(is_self)
-            def _():
-                local.start()
+            chunk_wait(s, d2d_rs.at[k_up - 1, s])
+        last = [(z - k_up, s, core) for s in range(subs) for core in range(2)]
+        update(last, order=(1, 0), between=lambda: send_attended(1))
+
+    @pl.when(z < k_up)
+    def _():
+        send_attended(1)
+
+    send_attended(0)
+
+    tok_gather.drain()
+    for i in range(2):
+
+        @pl.when(2 * c + i != y)
+        def _():
+            for n, sent in enumerate((kv_send.at[i], q_send.at[i], gate_send.at[i])):
+                pltpu.make_async_copy(sent, sent, a2a_ss.at[n, i]).wait()
+
+    @pl.when(c == 0)
+    def _():
+        for s in range(subs):
+            chunk_wait(s, own_ss.at[s])
+
+    @pl.loop(1, k_up + 1)
+    def _(k):
+        for d in range(2):
+            for s in range(subs):
+                more = jnp.logical_not(sends(d, k + 1, s))
+
+                @pl.when(jnp.logical_and(sends(d, k, s), more))
+                def _():
+                    chunk_wait(s, ring_ss.at[d, s])
+
+                more = jnp.logical_not(needs(d, k + 1, s))
+
+                @pl.when(jnp.logical_and(needs(d, k, s), more))
+                def _():
+                    chunk_wait(s, d2d_ss.at[d, s])
 
     wout_gather.finish_own()
-    wout_gather.finish_near()
+    wout_gather.finish_right()
+    wout_gather.finish_left()
     wout_gather.finish_far()
     cols = 256
     for n, dx in enumerate((0, 1, -1, 2)):
@@ -634,36 +671,7 @@
             else:
                 out_ref[:, span] = acc.astype(BF16)
 
-    tok_gather.drain()
     wout_gather.drain()
-    for i in range(2):
-
-        @pl.when(2 * c + i != y)
-        def _():
-            for n, sent in enumerate((kv_send.at[i], q_send.at[i], gate_send.at[i])):
-                pltpu.make_async_copy(sent, sent, a2a_ss.at[n, i]).wait()
-
-    @pl.when(c == 0)
-    def _():
-        for s in range(subs):
-            chunk_wait(s, own_ss.at[s])
-
-    @pl.loop(1, k_up + 1)
-    def _(k):
-        for d in range(2):
-            for s in range(subs):
-                more = jnp.logical_not(sends(d, k + 1, s))
-
-                @pl.when(jnp.logical_and(sends(d, k, s), more))
-                def _():
-                    chunk_wait(s, ring_ss.at[d, s])
-
-                more = jnp.logical_not(needs(d, k + 1, s))
-
-                @pl.when(jnp.logical_and(needs(d, k, s), more))
-                def _():
-                    chunk_wait(s, d2d_ss.at[d, s])
-
     stays = owner_core == c
     pieces = att_send.shape[0]
 
@@ -733,7 +741,7 @@
             dma((2, 2)),
             dma((2, k_up, 2)),
             dma((2, 2)),
-            dma((2, k_up, 2)),
+            dma((k_up, 2)),
             dma((2,)),
             dma((2,)),
             dma,

time: 66.6 us -> 66.1 us (level)
  no operation moved by 1% of the time
where the time goes in v6:
time: 66.1 us; the launch traced here: 66 us
  Pallas kernels  65.3 us (99%)
  local copies, waits for them, and re-layouts  0.68 us (1%)
    pallas_call x1, Pallas kernels, on_device(): pl.pallas_call(functools.partial(kernel, nz), out_shape=pltpu.VMEM((rows_...  65.3 us

profile of v6, /device:TPU:353, one launch (start us, length us, event | category | flops | bytes accessed | tf_op | source)
XLA Modules:
  0.0 66.0 jit_solution(161820205903978488)
XLA Ops:
  0.0 65.3 %shard_map.82 = bf16[48,2048]{1,0:T(8,128)(2,1)S(1)} custom-call(bf16[48,2048]{1,0:T(8,128)(2,1)} %tokens_ref.1, bf16[2048,128]{1,0:T(8,128)(2,1)} %wq_ref.1, bf16[2048,128]{1,0:T(8,128)(2,1)} %wk_ref.1, bf16[2048,128]{1,0:T(8,128)(2,1)} %wv_ref.1, f32[1,64]{1,0:T(1,128)} %bitcast.4, f32[1,64]{1,0:T(1,128)} %bitcast.5, f32[2,384]{1,0:T(2,128)} %bitcast.3, ...), custom_call_target="tpu_custom_call" | custom-call | tf_op jit(solution)/shard_map/pallas_call | solution.py:707
  65.3 0.7 %copy.10 = bf16[48,2048]{1,0:T(8,128)(2,1)} copy(bf16[48,2048]{1,0:T(8,128)(2,1)S(1)} %shard_map.82) | data formatting | bytes 393216

commit v7 on v6

--- a/solution.py
+++ b/solution.py
@@ -130,6 +130,7 @@
     m_s,
     o_s,
     v_s,
+    k_s,
     att_send,
     att_recv,
     acc_s,
@@ -439,10 +440,9 @@
     def update(pieces, masked=False, order=tuple(range(half // QT)), between=None):
         count = len(pieces) * blk
 
-        def keys():
-            return jnp.concatenate([kv_all[b, s, core] for b, s, core in pieces], axis=0)
-
-        v_s[pl.ds(0, count), :] = keys() * keep_high + ones_low
+        joined = jnp.concatenate([kv_all[b, s, core] for b, s, core in pieces], axis=0)
+        v_s[pl.ds(0, count), :] = joined * keep_high + ones_low
+        k_s[:, pl.ds(0, count)] = jnp.transpose(joined)
         gate_row = jnp.concatenate(
             [
                 gate_all[b, core, pl.ds(s * tiles_blk + i, 1), :]
@@ -453,10 +453,9 @@
         )
 
         def score_of(t):
-            score = lax.dot_general(
-                q_s[pl.ds(t * QT, QT), :],
-                keys(),
-                (((1,), (1,)), ((), ())),
+            score = jnp.dot(
+                q_s[pl.ds(t * QT, QT), 0:HEAD],
+                k_s[0:HEAD, pl.ds(0, count)],
                 preferred_element_type=F32,
             )
             score = score - gate_row
@@ -728,6 +727,7 @@
             pltpu.VMEM((half, LANES), F32),
             pltpu.VMEM((half, LANES), F32),
             pltpu.VMEM((2 * half, LANES), BF16),
+            pltpu.VMEM((LANES, 2 * half), BF16),
             pltpu.VMEM((2 * NX * NC, rows_tp // 2, LANES), BF16),
             pltpu.VMEM((NX * NY, rows_tp // 2, LANES), BF16),
             pltpu.VMEM((rows_tp, output_weight.shape[1]), F32),

time: 66.1 us -> 65.7 us (level)
  no operation moved by 1% of the time
where the time goes in v7:
time: 65.7 us; the launch traced here: 65.6 us
  Pallas kernels  64.9 us (99%)
  local copies, waits for them, and re-layouts  0.68 us (1%)
    pallas_call x1, Pallas kernels, on_device(): pl.pallas_call(functools.partial(kernel, nz), out_shape=pltpu.VMEM((rows_...  64.9 us

profile of v7, /device:TPU:353, one launch (start us, length us, event | category | flops | bytes accessed | tf_op | source)
XLA Modules:
  0.0 65.6 jit_solution(12492975580423941276)
XLA Ops:
  0.0 64.9 %shard_map.82 = bf16[48,2048]{1,0:T(8,128)(2,1)S(1)} custom-call(bf16[48,2048]{1,0:T(8,128)(2,1)} %tokens_ref.1, bf16[2048,128]{1,0:T(8,128)(2,1)} %wq_ref.1, bf16[2048,128]{1,0:T(8,128)(2,1)} %wk_ref.1, bf16[2048,128]{1,0:T(8,128)(2,1)} %wv_ref.1, f32[1,64]{1,0:T(1,128)} %bitcast.4, f32[1,64]{1,0:T(1,128)} %bitcast.5, f32[2,384]{1,0:T(2,128)} %bitcast.3, ...), custom_call_target="tpu_custom_call" | custom-call | tf_op jit(solution)/shard_map/pallas_call | solution.py:706
  64.9 0.7 %copy.10 = bf16[48,2048]{1,0:T(8,128)(2,1)} copy(bf16[48,2048]{1,0:T(8,128)(2,1)S(1)} %shard_map.82) | data formatting | bytes 393216
